TPU v7x, 32 devices: a whole 2x2x4 slice. The times are simulated.
32 devices in a mesh: grp: 2 (over y), sp: 4 (over z), fs: 2 (over x), tp: 2 (over core).
Axes of the slice: x: 2, y: 2, z: 4, core: 2. Of those that a mesh axis runs over, the one named last changes fastest.
Arguments:
- tokens: bfloat16 [4, 512, 2048], P(('grp', 'fs'), 'sp', 'tp'), parts along dimension 0, may hold values from -120 to 120
- mix_gain: float32 [2048], replicated, may hold values from 0.1 to 1.9
- attn_query: bfloat16 [2048, 1024], P('fs', 'tp'), may hold values from -0.375 to 0.375
- attn_key: bfloat16 [2048, 1024], P('fs', 'tp'), may hold values from -0.125 to 0.125
- attn_value: bfloat16 [2048, 1024], P('fs', 'tp'), may hold values from -0.125 to 0.125
- rec_query: bfloat16 [2048, 1024], P('fs', 'tp'), may hold values from -0.125 to 0.125
- rec_forget: bfloat16 [2048, 1024], P('fs', 'tp'), may hold values from -0.125 to 0.125
- rec_input: bfloat16 [2048, 1024], P('fs', 'tp'), may hold values from -0.125 to 0.125
- break_offset: float32 [8], P('tp'), may hold values from -13.5 to -7
- forget_room: float32 [8, 128], P('tp'), may hold values from 0.0009765625 to 0.05
- out_gain: float32 [128], replicated, may hold values from 0.1 to 1.9
- out_attn: bfloat16 [1024, 2048], P('tp', 'fs'), may hold values from -0.125 to 0.125
- out_rec: bfloat16 [1024, 2048], P('tp', 'fs'), may hold values from -0.125 to 0.125
Outputs:
- mixed: bfloat16 [4, 512, 2048], P(('grp', 'fs'), ('sp', 'tp')), parts along dimension 0
There are 2 independent parts, one for each index of `grp`. A program takes and returns all parts, laid end to end along the dimension named above; an argument that names none is the same for every part. Nothing has to cross between parts.
All inputs are finite; a program needn't handle non-finite values.
Results may differ from a plain program's by a relative error of at most 0.019.
Values may be sent and summed in bfloat16 or wider, within the bound.
A program may use at most 64 MiB of HBM per device.

v0:
```python
import math

import jax
import jax.numpy as jnp
from jax import lax
from jax.sharding import PartitionSpec as P

HEAD = 128
DK = 128
DV = 128
REC_BLOCK = 64


norm_eps = 1e-06
highest = lax.Precision.HIGHEST


def carried_in(x, axis, join, neutral):
    place = lax.axis_index(axis)
    gathered = jax.tree.map(
        lambda a, kind: lax.all_gather(a.astype(kind), axis), x, (jnp.bfloat16, jnp.bfloat16)
    )
    state = jax.tree.map(lambda a, e: jnp.zeros_like(a) + jnp.asarray(e, a.dtype), x, neutral)

    def one(step, state):
        return join(
            state,
            jax.tree.map(
                lambda a, own: lax.dynamic_index_in_dim(a, step, 0, False).astype(own.dtype),
                gathered,
                x,
            ),
        )

    return lax.fori_loop(0, place, one, state)


def block_step(states, inputs):
    queries, key_in, value_rows, log_forget = inputs
    block_len = queries.shape[-2]
    cum_log = jnp.cumsum(log_forget, axis=-2)
    last_log = cum_log[..., -1:, :]
    q_dec = queries * jnp.exp(cum_log)
    k_inv = key_in * jnp.exp(-cum_log)
    causal = lax.iota(jnp.int32, block_len)[:, None] >= lax.iota(jnp.int32, block_len)[None, :]
    carried_part = jnp.einsum("...tk,...kv->...tv", q_dec, states, precision=highest)
    scores = jnp.where(
        causal, jnp.einsum("...tk,...sk->...ts", q_dec, k_inv, precision=highest), 0.0
    )
    inner_part = jnp.einsum("...ts,...sv->...tv", scores, value_rows, precision=highest)
    fresh_state = jnp.einsum(
        "...sk,...sv->...kv", key_in * jnp.exp(last_log - cum_log), value_rows, precision=highest
    )
    return (
        jnp.exp(jnp.swapaxes(last_log, -1, -2)) * states + fresh_state,
        carried_part + inner_part,
    )


def stick_mixer(queries, key_rows, value_rows, offsets):
    seq_count, tok_rows, head_count, head_width = queries.shape
    own_index = lax.axis_index("sp")
    sp_count = lax.axis_size("sp")
    factor = 1.0 / math.sqrt(head_width)
    q_pos = own_index * tok_rows + lax.iota(jnp.int32, tok_rows)
    start_acc = jnp.zeros((sp_count, seq_count, tok_rows, head_count, head_width), jnp.float32)
    start_log = jnp.zeros((sp_count, seq_count, tok_rows, head_count), jnp.float32)

    def one_block(carried, key_blk, value_blk, slot):

        def compute(states):
            sums_acc, log_sums = states
            scores = jnp.einsum(
                "bqhe,bkhe->bhqk", queries, key_blk, preferred_element_type=jnp.float32
            )
            scores = scores * factor + offsets[None, :, None, None]
            k_pos = slot * tok_rows + lax.iota(jnp.int32, tok_rows)
            strict = k_pos[None, :] < q_pos[:, None]
            log_keep = jnp.where(strict, jax.nn.log_sigmoid(-scores), 0.0)
            inner_sum = lax.cumsum(log_keep, axis=3, reverse=True) - log_keep
            sticks = jnp.where(strict, jnp.exp(jax.nn.log_sigmoid(scores) + inner_sum), 0.0).astype(
                jnp.bfloat16
            )
            partial_value = jnp.einsum(
                "bhqk,bkhe->bqhe", sticks, value_blk, preferred_element_type=jnp.float32
            )
            totals = jnp.transpose(jnp.sum(log_keep, axis=3), (0, 2, 1))
            return (
                lax.dynamic_update_index_in_dim(sums_acc, partial_value, slot, 0),
                lax.dynamic_update_index_in_dim(log_sums, totals, slot, 0),
            )

        return lax.cond(slot <= own_index, compute, lambda states: states, carried)

    key_all = lax.all_gather(key_rows, "sp", axis=1, tiled=True)
    value_all = lax.all_gather(value_rows, "sp", axis=1, tiled=True)
    blocks = key_all.shape[1] // tok_rows

    def turn(block_idx, states):
        key_blk = lax.dynamic_slice_in_dim(key_all, block_idx * tok_rows, tok_rows, 1)
        value_blk = lax.dynamic_slice_in_dim(value_all, block_idx * tok_rows, tok_rows, 1)
        return one_block(states, key_blk, value_blk, block_idx)

    sums_acc, log_sums = lax.fori_loop(0, blocks, turn, (start_acc, start_log))
    later_sum = jnp.cumsum(log_sums[::-1], axis=0)[::-1] - log_sums
    return jnp.sum(sums_acc * jnp.exp(later_sum)[..., None], axis=0).astype(jnp.bfloat16)


def combine_states(earlier, later):
    return (earlier[0] + later[0], jnp.exp(later[0])[..., None] * earlier[1] + later[1])


def recur_mixer(queries, gate_pre, inputs, rooms, gain):
    seq_count, tok_rows, head_count, key_dim = queries.shape
    val_dim = inputs.shape[3]
    key_in = rooms * jax.nn.sigmoid(-gate_pre.astype(jnp.float32))
    log_forget = jnp.log1p(-key_in)
    query32 = queries.astype(jnp.float32)
    blocks = tok_rows // REC_BLOCK

    def split_blocks(tensor):
        return jnp.transpose(
            tensor.reshape(seq_count, blocks, REC_BLOCK, head_count, tensor.shape[3]),
            (1, 0, 3, 2, 4),
        )

    empty_state = jnp.zeros((seq_count, head_count, key_dim, val_dim), jnp.float32)
    final_state, pieces = lax.scan(
        block_step,
        empty_state,
        (
            split_blocks(query32),
            split_blocks(key_in),
            split_blocks(inputs.astype(jnp.float32)),
            split_blocks(log_forget),
        ),
    )
    local_out = jnp.transpose(pieces, (1, 0, 3, 2, 4)).reshape(
        seq_count, tok_rows, head_count, val_dim
    )
    running = jnp.cumsum(log_forget, axis=1)
    identity = (jnp.zeros((seq_count, head_count, key_dim), jnp.float32), empty_state)
    incoming = carried_in((running[:, -1], final_state), "sp", combine_states, identity)[1]
    raw_out = local_out + jnp.einsum(
        "bthk,bhkv->bthv", query32 * jnp.exp(running), incoming, precision=highest
    )
    factor = lax.rsqrt(jnp.mean(raw_out * raw_out, axis=3, keepdims=True) + norm_eps)
    return (raw_out * factor * gain).astype(jnp.bfloat16)


def body(
    tokens,
    mix_gain,
    attn_query,
    attn_key,
    attn_value,
    rec_query,
    rec_forget,
    rec_input,
    break_offset,
    forget_room,
    out_gain,
    out_attn,
    out_rec,
):
    whole = lax.all_gather(tokens, "tp", axis=2, tiled=True)
    seq_rows = whole.shape[1]
    model_width = whole.shape[2]
    rows32 = whole.astype(jnp.float32)
    factor = lax.rsqrt(jnp.mean(rows32 * rows32, axis=2, keepdims=True) + norm_eps)
    normed = (rows32 * factor * mix_gain).astype(jnp.bfloat16).reshape(seq_rows, model_width)
    weights = (attn_query, attn_key, attn_value, rec_query, rec_forget, rec_input)
    turned = (
        lax.all_to_all(weights[0], "fs", split_axis=1, concat_axis=0, tiled=True),
        lax.all_to_all(weights[1], "fs", split_axis=1, concat_axis=0, tiled=True),
        lax.all_to_all(weights[2], "fs", split_axis=1, concat_axis=0, tiled=True),
        lax.all_to_all(weights[3], "fs", split_axis=1, concat_axis=0, tiled=True),
        lax.all_to_all(weights[4], "fs", split_axis=1, concat_axis=0, tiled=True),
        lax.all_to_all(weights[5], "fs", split_axis=1, concat_axis=0, tiled=True),
    )
    pieces = lax.all_gather(normed, "fs", axis=0, tiled=True)
    projected = tuple(
        (
            jnp.dot(pieces, matrix, preferred_element_type=jnp.float32).astype(jnp.bfloat16)
            for matrix in turned
        )
    )
    seq_count = lax.axis_size("fs")
    own_fs = lax.axis_index("fs")
    attn_heads = break_offset.shape[0] // seq_count
    rec_heads = forget_room.shape[0] // seq_count
    offsets = lax.dynamic_slice_in_dim(break_offset, own_fs * attn_heads, attn_heads, 0)
    rooms = lax.dynamic_slice_in_dim(forget_room, own_fs * rec_heads, rec_heads, 0)

    def heads_of(matrix, width_each):
        return matrix.reshape(seq_count, seq_rows, matrix.shape[1] // width_each, width_each)

    attn_out = stick_mixer(
        heads_of(projected[0], HEAD),
        heads_of(projected[1], HEAD),
        heads_of(projected[2], HEAD),
        offsets,
    )
    rec_out = recur_mixer(
        heads_of(projected[3], DK),
        heads_of(projected[4], DK),
        heads_of(projected[5], DV),
        rooms,
        out_gain,
    )
    attn_flat = attn_out.reshape(seq_count * seq_rows, -1)
    rec_flat = rec_out.reshape(seq_count * seq_rows, -1)
    attn_flat, rec_flat = (
        lax.all_to_all(attn_flat, "fs", split_axis=0, concat_axis=1, tiled=True),
        lax.all_to_all(rec_flat, "fs", split_axis=0, concat_axis=1, tiled=True),
    )
    full_attn, full_rec = (
        lax.all_gather(out_attn, "fs", axis=1, tiled=True),
        lax.all_gather(out_rec, "fs", axis=1, tiled=True),
    )
    share = seq_rows // lax.axis_size("tp")
    mixed = lax.psum_scatter(
        (
            jnp.dot(attn_flat, full_attn, preferred_element_type=jnp.float32)
            + jnp.dot(rec_flat, full_rec, preferred_element_type=jnp.float32)
        ).astype(jnp.bfloat16),
        "tp",
        scatter_dimension=0,
        tiled=True,
    )
    return mixed.reshape(1, share, model_width)


def solution(mesh):
    placed = (
        P(("grp", "fs"), "sp", "tp"),
        P(),
        P("fs", "tp"),
        P("fs", "tp"),
        P("fs", "tp"),
        P("fs", "tp"),
        P("fs", "tp"),
        P("fs", "tp"),
        P("tp"),
        P("tp", None),
        P(),
        P("tp", "fs"),
        P("tp", "fs"),
    )
    return jax.shard_map(
        body,
        mesh=mesh,
        in_specs=placed,
        out_specs=P(("grp", "fs"), ("sp", "tp"), None),
        check_vma=False,
    )
```

profile of v0, /device:TPU:29, one launch (start us, length us, event | category | flops | bytes accessed | tf_op | source)
XLA Modules:
  0.0 284.5 jit_solution(8007163119693888808)
XLA Ops:
  6.5 2.8 all_gather.28
  9.6 1.7 fusion.54
  11.3 1.3 copy.92
  12.6 3.6 %all-to-all-start.4 = ((bf16[1024,2,256]{0,2,1:T(8,128)(2,1)}), bf16[1024,2,256]{0,2,1:T(8,128)(2,1)S(1)}, u32[]{:S(2)}, u32[]{:S(2)}) async-start(bf16[1024,2,256]{0,2,1:T(8,128)(2,1)} %bitcast.20), calls=%async_computation.4 | async-start | bytes 2097152 | tf_op jit(solution)/shard_map/all_to_all | solution.py:178
  16.2 1.3 copy.98
  17.5 19.4 %all-to-all-done.4 = bf16[1024,2,256]{0,2,1:T(8,128)(2,1)S(1)} async-done(((bf16[1024,2,256]{0,2,1:T(8,128)(2,1)}), bf16[1024,2,256]{0,2,1:T(8,128)(2,1)S(1)}, u32[]{:S(2)}, u32[]{:S(2)}) %all-to-all-start.4) | async-done | bytes 1048608 | tf_op jit(solution)/shard_map/all_to_all | solution.py:178
  36.9 3.6 %all-to-all-start.6 = ((bf16[1024,2,256]{0,2,1:T(8,128)(2,1)}), bf16[1024,2,256]{0,2,1:T(8,128)(2,1)S(1)}, u32[]{:S(2)}, u32[]{:S(2)}) async-start(bf16[1024,2,256]{0,2,1:T(8,128)(2,1)} %bitcast.29), calls=%async_computation.6 | async-start | bytes 2097152 | tf_op jit(solution)/shard_map/all_to_all | solution.py:177
  41.3 1.3 copy.95
  42.6 8.8 %all-to-all-done.6 = bf16[1024,2,256]{0,2,1:T(8,128)(2,1)S(1)} async-done(((bf16[1024,2,256]{0,2,1:T(8,128)(2,1)}), bf16[1024,2,256]{0,2,1:T(8,128)(2,1)S(1)}, u32[]{:S(2)}, u32[]{:S(2)}) %all-to-all-start.6) | async-done | bytes 1048608 | tf_op jit(solution)/shard_map/all_to_all | solution.py:177
  51.4 3.6 %all-to-all-start.5 = ((bf16[1024,2,256]{0,2,1:T(8,128)(2,1)}), bf16[1024,2,256]{0,2,1:T(8,128)(2,1)S(1)}, u32[]{:S(2)}, u32[]{:S(2)}) async-start(bf16[1024,2,256]{0,2,1:T(8,128)(2,1)} %bitcast.144), calls=%async_computation.5 | async-start | bytes 2097152 | tf_op jit(solution)/shard_map/all_to_all | solution.py:179
  55.0 2.3 copy.82
  57.3 21.6 %all-to-all-done.5 = bf16[1024,2,256]{0,2,1:T(8,128)(2,1)S(1)} async-done(((bf16[1024,2,256]{0,2,1:T(8,128)(2,1)}), bf16[1024,2,256]{0,2,1:T(8,128)(2,1)S(1)}, u32[]{:S(2)}, u32[]{:S(2)}) %all-to-all-start.5) | async-done | bytes 1048608 | tf_op jit(solution)/shard_map/all_to_all | solution.py:179
  78.9 4.4 %all-to-all-start = ((bf16[1024,2,256]{0,2,1:T(8,128)(2,1)}), bf16[1024,2,256]{0,2,1:T(8,128)(2,1)}, u32[]{:S(2)}, u32[]{:S(2)}) async-start(bf16[1024,2,256]{0,2,1:T(8,128)(2,1)} %bitcast.145), calls=%async_computation | async-start | bytes 2097152 | tf_op jit(solution)/shard_map/all_to_all | solution.py:175
  83.3 2.3 copy.87
  85.6 14.9 %all-to-all-done = bf16[1024,2,256]{0,2,1:T(8,128)(2,1)} async-done(((bf16[1024,2,256]{0,2,1:T(8,128)(2,1)}), bf16[1024,2,256]{0,2,1:T(8,128)(2,1)}, u32[]{:S(2)}, u32[]{:S(2)}) %all-to-all-start) | async-done | bytes 1048608 | tf_op jit(solution)/shard_map/all_to_all | solution.py:175
  100.5 4.5 %all-to-all-start.2 = ((bf16[1024,2,256]{0,2,1:T(8,128)(2,1)}), bf16[1024,2,256]{0,2,1:T(8,128)(2,1)}, u32[]{:S(2)}, u32[]{:S(2)}) async-start(bf16[1024,2,256]{0,2,1:T(8,128)(2,1)} %bitcast.146), calls=%async_computation.2 | async-start | bytes 2097152 | tf_op jit(solution)/shard_map/all_to_all | solution.py:176
  105.0 2.3 copy.85
  107.3 9.5 %all-to-all-done.2 = bf16[1024,2,256]{0,2,1:T(8,128)(2,1)} async-done(((bf16[1024,2,256]{0,2,1:T(8,128)(2,1)}), bf16[1024,2,256]{0,2,1:T(8,128)(2,1)}, u32[]{:S(2)}, u32[]{:S(2)}) %all-to-all-start.2) | async-done | bytes 1048608 | tf_op jit(solution)/shard_map/all_to_all | solution.py:176
  116.7 4.4 %all-to-all-start.1 = ((bf16[1024,2,256]{0,2,1:T(8,128)(2,1)}), bf16[1024,2,256]{0,2,1:T(8,128)(2,1)}, u32[]{:S(2)}, u32[]{:S(2)}) async-start(bf16[1024,2,256]{0,2,1:T(8,128)(2,1)} %bitcast.141), calls=%async_computation.1 | async-start | bytes 2097152 | tf_op jit(solution)/shard_map/all_to_all | solution.py:174
  122.0 1.3 copy.93
  123.4 1.3 copy.99
  124.7 1.4 copy.96
  126.0 2.3 copy.83
  128.3 2.4 copy.88
  130.6 1.4 all-to-all-done.1
  132.0 1.5 copy.86
  133.6 2.6 fusion.51
  136.1 1.8 div.26
  138.0 1.9 div.27
  139.9 2.4 fusion.46
  142.3 1.8 reshape.147
  144.0 1.8 reshape.145
  145.8 1.2 fusion.47
  148.0 1.8 fusion.66
  150.8 6.9 %while.43 = (s32[]{:T(128)}, f32[2,2,128,128]{3,2,1,0:T(8,128)S(1)}, f32[2,2,2,64,128]{4,3,0,2,1:T(8,128)}, f32[2,2,2,64,128]{4,3,2,1,0:T(8,128)}, f32[2,2,2,64,...) while((s32[]{:T(128)}, ...), condition=%wide.region_11.12_spmd.clone, body=%wide.region_9.11_spmd.clone.sunk | while | flops 153571328 | bytes 3239036 | solution.py:128
  157.7 14.6 %all-gather.2 = bf16[8,2,128,128]{3,2,1,0:T(8,128)(2,1)} all-gather(bf16[2,2,128,128]{3,2,1,0:T(8,128)(2,1)S(1)} %convert_element_type.118), channel_id=4, replica_groups=mesh['grp'=2,'sp'=4,'fs'=2,'tp'=2] {'sp'}, dimensions={0}, use_global_device_ids=true | all-gather | bytes 655360 | tf_op jit(solution)/shard_map/all_gather | solution.py:21
  172.4 2.3 exponential_multiply_fusion
  174.7 5.7 %all-gather.1 = bf16[8,1,2,128]{3,2,1,0:T(2,128)(2,1)S(1)} all-gather(bf16[2,1,2,128]{3,2,1,0:T(2,128)(2,1)S(1)} %slice.12), channel_id=3, replica_groups=mesh['grp'=2,'sp'=4,'fs'=2,'tp'=2] {'sp'}, dimensions={0}, use_global_device_ids=true | all-gather | bytes 5120 | tf_op jit(solution)/shard_map/all_gather | solution.py:21
  180.4 1.8 copy.104
  182.2 1.7 convolution_convert_fusion.5
  183.9 13.9 %all_gather.30 = bf16[2,512,2,128]{3,1,2,0:T(8,128)(2,1)} all-gather(bf16[2,128,2,128]{3,1,2,0:T(8,128)(2,1)S(1)} %copy.84), channel_id=1, replica_groups=mesh['grp'=2,'sp'=4,'fs'=2,'tp'=2] {'sp'}, dimensions={1}, use_global_device_ids=true | all-gather | bytes 655360 | tf_op jit(solution)/shard_map/all_gather | solution.py:95
  198.3 13.9 %all_gather.31 = bf16[2,512,2,128]{3,1,2,0:T(8,128)(2,1)S(1)} all-gather(bf16[2,128,2,128]{3,1,2,0:T(8,128)(2,1)S(1)} %copy.89), channel_id=1, replica_groups=mesh['grp'=2,'sp'=4,'fs'=2,'tp'=2] {'sp'}, dimensions={1}, use_global_device_ids=true | all-gather | bytes 655360 | tf_op jit(solution)/shard_map/all_gather | solution.py:96
  212.8 25.9 %while.42 = (s32[]{:T(128)}, f32[4,2,128,2,128]{4,2,3,1,0:T(8,128)S(1)}, f32[4,2,128,2]{2,3,1,0:T(2,128)S(1)}, s32[]{:T(128)}, bf16[2,512,2,128]{3,1,2,0:T(8,128...) while((s32[]{:T(128)}, ...), condition=%wide.region_6.7_spmd.clone, body=%wide.region_1.6_spmd.clone.sunk | while | flops 43925260 | bytes 2286935 | solution.py:104
  212.9 6.4 %conditional.3 = ((f32[4,2,128,2,128]{4,2,3,1,0:T(8,128)S(1)}, f32[4,2,128,2]{2,3,1,0:T(2,128)S(1)})) conditional(s32[]{:T(128)} %convert_element_type.168, (f32[4,2,128,2,128]{4,2,3,1,0:T(8,128)S(1)}, f32[4,2,128,2]{2,3,1,0:T(2,128)S(1)}) %tuple.100, (s32[]{:T(128)}, s32[]{:T(128)}, bf16[2,512,2,128]{3,1,2,0:T(8,128)(2,1)}, ...), branch_computations={%region_2.0_spmd, %region_3.5_spmd} | conditional | flops 43925256 | bytes 2286220 | solution.py:93
  213.0 1.3 fusion.20
  214.3 4.4 %reduce_window_sum.43 = f32[2,2,128,128]{2,3,1,0:T(8,128)S(1)} reduce-window(f32[2,2,128,128]{2,3,1,0:T(8,128)S(1)} %get-tuple-element.514, f32[]{:T(128)} %constant.131.clone), window={size=1x1x1x128 pad=0_0x0_0x0_0x0_127}, to_apply=%region_4.3 | reduce-window | flops 8323072 | bytes 524292 | tf_op jit(solution)/shard_map/while/body/eval_jaxpr/cond/branch_1_fun/reduce_window_sum | solution.py:80
  219.3 6.4 %conditional.3 = ((f32[4,2,128,2,128]{4,2,3,1,0:T(8,128)S(1)}, f32[4,2,128,2]{2,3,1,0:T(2,128)S(1)})) conditional(s32[]{:T(128)} %convert_element_type.168, (f32[4,2,128,2,128]{4,2,3,1,0:T(8,128)S(1)}, f32[4,2,128,2]{2,3,1,0:T(2,128)S(1)}) %tuple.100, (s32[]{:T(128)}, s32[]{:T(128)}, bf16[2,512,2,128]{3,1,2,0:T(8,128)(2,1)}, ...), branch_computations={%region_2.0_spmd, %region_3.5_spmd} | conditional | flops 43925256 | bytes 2286220 | solution.py:93
  219.5 1.3 fusion.20
  220.8 4.4 %reduce_window_sum.43 = f32[2,2,128,128]{2,3,1,0:T(8,128)S(1)} reduce-window(f32[2,2,128,128]{2,3,1,0:T(8,128)S(1)} %get-tuple-element.514, f32[]{:T(128)} %constant.131.clone), window={size=1x1x1x128 pad=0_0x0_0x0_0x0_127}, to_apply=%region_4.3 | reduce-window | flops 8323072 | bytes 524292 | tf_op jit(solution)/shard_map/while/body/eval_jaxpr/cond/branch_1_fun/reduce_window_sum | solution.py:80
  225.8 6.4 %conditional.3 = ((f32[4,2,128,2,128]{4,2,3,1,0:T(8,128)S(1)}, f32[4,2,128,2]{2,3,1,0:T(2,128)S(1)})) conditional(s32[]{:T(128)} %convert_element_type.168, (f32[4,2,128,2,128]{4,2,3,1,0:T(8,128)S(1)}, f32[4,2,128,2]{2,3,1,0:T(2,128)S(1)}) %tuple.100, (s32[]{:T(128)}, s32[]{:T(128)}, bf16[2,512,2,128]{3,1,2,0:T(8,128)(2,1)}, ...), branch_computations={%region_2.0_spmd, %region_3.5_spmd} | conditional | flops 43925256 | bytes 2286220 | solution.py:93
  225.9 1.3 fusion.20
  227.2 4.4 %reduce_window_sum.43 = f32[2,2,128,128]{2,3,1,0:T(8,128)S(1)} reduce-window(f32[2,2,128,128]{2,3,1,0:T(8,128)S(1)} %get-tuple-element.514, f32[]{:T(128)} %constant.131.clone), window={size=1x1x1x128 pad=0_0x0_0x0_0x0_127}, to_apply=%region_4.3 | reduce-window | flops 8323072 | bytes 524292 | tf_op jit(solution)/shard_map/while/body/eval_jaxpr/cond/branch_1_fun/reduce_window_sum | solution.py:80
  232.3 6.4 %conditional.3 = ((f32[4,2,128,2,128]{4,2,3,1,0:T(8,128)S(1)}, f32[4,2,128,2]{2,3,1,0:T(2,128)S(1)})) conditional(s32[]{:T(128)} %convert_element_type.168, (f32[4,2,128,2,128]{4,2,3,1,0:T(8,128)S(1)}, f32[4,2,128,2]{2,3,1,0:T(2,128)S(1)}) %tuple.100, (s32[]{:T(128)}, s32[]{:T(128)}, bf16[2,512,2,128]{3,1,2,0:T(8,128)(2,1)}, ...), branch_computations={%region_2.0_spmd, %region_3.5_spmd} | conditional | flops 43925256 | bytes 2286220 | solution.py:93
  232.4 1.3 fusion.20
  233.7 4.4 %reduce_window_sum.43 = f32[2,2,128,128]{2,3,1,0:T(8,128)S(1)} reduce-window(f32[2,2,128,128]{2,3,1,0:T(8,128)S(1)} %get-tuple-element.514, f32[]{:T(128)} %constant.131.clone), window={size=1x1x1x128 pad=0_0x0_0x0_0x0_127}, to_apply=%region_4.3 | reduce-window | flops 8323072 | bytes 524292 | tf_op jit(solution)/shard_map/while/body/eval_jaxpr/cond/branch_1_fun/reduce_window_sum | solution.py:80
  239.9 3.4 %all-to-all-start.3 = ((bf16[2,128,256]{1,2,0:T(8,128)(2,1)}), bf16[2,128,256]{1,2,0:T(8,128)(2,1)S(1)}, u32[]{:S(2)}, u32[]{:S(2)}) async-start(bf16[2,128,256]{1,2,0:T(8,128)(2,1)} %bitcast.17), calls=%async_computation.3 | async-start | bytes 262144 | tf_op jit(solution)/shard_map/all_to_all | solution.py:214
  243.3 3.4 %while.41 = (s32[]{:T(128)}, f32[2,2,128,128]{3,2,1,0:T(8,128)S(1)}, s32[]{:T(128)}, bf16[4,2,2,128]{3,2,1,0:T(2,128)(2,1)S(1)}, bf16[4,2,2,128,128]{4,3,2,1,0:T(8,128)(2,1)}, /*index=5*/s32[]{:T(128)}, s32[]{:T(128)}, s32[]{:T(128)}) while((s32[]{:T(128)}, f32[2,2,128,128]{3,2,1,0:T(8,128)S(1)}, s32[]{:T(128)}, ...), condition=%wide.region_14.15_spmd, body=%wide.region_13.14_spmd.sunk | while | flops 197125 | bytes 660607 | solution.py:35
  243.4 1.1 convert_add_fusion.2
  244.5 1.1 convert_add_fusion.2
  248.2 3.4 %all-to-all-start.7 = ((bf16[2,128,256]{1,2,0:T(8,128)(2,1)}), bf16[2,128,256]{1,2,0:T(8,128)(2,1)S(1)}, u32[]{:S(2)}, u32[]{:S(2)}) async-start(bf16[2,128,256]{1,2,0:T(8,128)(2,1)} %bitcast.38), calls=%async_computation.7 | async-start | bytes 262144 | tf_op jit(solution)/shard_map/all_to_all | solution.py:215
  251.6 2.1 fusion.69
  253.7 1.2 all-to-all-done.7
  254.9 2.9 %fusion.44 = bf16[128,2048]{1,0:T(8,128)(2,1)} fusion(f32[128,2048]{1,0:T(8,128)S(1)} %fusion.69, bf16[128,512]{0,1:T(8,128)(2,1)S(1)} %bitcast.150, bf16[512,2048]{1,0:T(8,128)(2,1)} %all-gather.9.cloned.1.call-done), kind=kOutput, calls=%fused_computation.60 | convolution fusion | flops 268959744 | bytes 3801088 | tf_op jit(solution)/shard_map/dot_general | solution.py:225
  257.7 20.3 %reduce-scatter.2.cloned.1.call-done = bf16[64,2048]{1,0:T(8,128)(2,1)} async-done(((bf16[128,2048]{1,0:T(8,128)(2,1)}), bf16[64,2048]{1,0:T(8,128)(2,1)}) %reduce-scatter.2.cloned.1.call-update) | async-done | bytes 262160 | tf_op jit(solution)/shard_map/reduce_scatter | solution.py:222
  (107 shorter events, 18.3 us)
Async XLA Ops:
  6.5 115.5 %copy-start = (f32[4,128]{1,0:T(4,128)S(1)}, f32[4,128]{1,0:T(4,128)}, u32[]{:S(2)}) copy-start(f32[4,128]{1,0:T(4,128)} %param.30) | copy-start | bytes 6148
  6.5 4.7 %copy-start.4 = (bf16[1024,512]{1,0:T(8,128)(2,1)S(1)}, bf16[1024,512]{1,0:T(8,128)(2,1)}, u32[]{:S(2)}) copy-start(bf16[1024,512]{1,0:T(8,128)(2,1)} %param.27) | copy-start | bytes 3145732
  6.5 127.0 %all-gather.11.cloned.1.call-start = ((), (), s32[]{:S(2)}) async-start(), calls=%async_computation.12 | async-start | bytes 1572864 | tf_op jit(solution)/shard_map/all_gather | solution.py:181
  11.3 4.9 %copy-start.5 = (bf16[1024,512]{1,0:T(8,128)(2,1)S(1)}, bf16[1024,512]{1,0:T(8,128)(2,1)}, u32[]{:S(2)}) copy-start(bf16[1024,512]{1,0:T(8,128)(2,1)} %param.26) | copy-start | bytes 3145732
  12.6 24.3 %all-to-all-start.4 = ((bf16[1024,2,256]{0,2,1:T(8,128)(2,1)}), bf16[1024,2,256]{0,2,1:T(8,128)(2,1)S(1)}, u32[]{:S(2)}, u32[]{:S(2)}) async-start(bf16[1024,2,256]{0,2,1:T(8,128)(2,1)} %bitcast.20), calls=%async_computation.4 | async-start | bytes 2097152 | tf_op jit(solution)/shard_map/all_to_all | solution.py:178
  17.5 23.7 %copy-start.6 = (bf16[1024,512]{1,0:T(8,128)(2,1)S(1)}, bf16[1024,512]{1,0:T(8,128)(2,1)}, u32[]{:S(2)}) copy-start(bf16[1024,512]{1,0:T(8,128)(2,1)} %param.28) | copy-start | bytes 3145732
  36.9 14.5 %all-to-all-start.6 = ((bf16[1024,2,256]{0,2,1:T(8,128)(2,1)}), bf16[1024,2,256]{0,2,1:T(8,128)(2,1)S(1)}, u32[]{:S(2)}, u32[]{:S(2)}) async-start(bf16[1024,2,256]{0,2,1:T(8,128)(2,1)} %bitcast.29), calls=%async_computation.6 | async-start | bytes 2097152 | tf_op jit(solution)/shard_map/all_to_all | solution.py:177
  40.5 211.1 %all-gather.7.cloned.1.call-start = ((), (), s32[]{:S(2)}) async-start(), calls=%async_computation.9 | async-start | bytes 3145728 | tf_op jit(solution)/shard_map/all_gather | solution.py:218
  51.4 27.5 %all-to-all-start.5 = ((bf16[1024,2,256]{0,2,1:T(8,128)(2,1)}), bf16[1024,2,256]{0,2,1:T(8,128)(2,1)S(1)}, u32[]{:S(2)}, u32[]{:S(2)}) async-start(bf16[1024,2,256]{0,2,1:T(8,128)(2,1)} %bitcast.144), calls=%async_computation.5 | async-start | bytes 2097152 | tf_op jit(solution)/shard_map/all_to_all | solution.py:179
  78.9 21.6 %all-to-all-start = ((bf16[1024,2,256]{0,2,1:T(8,128)(2,1)}), bf16[1024,2,256]{0,2,1:T(8,128)(2,1)}, u32[]{:S(2)}, u32[]{:S(2)}) async-start(bf16[1024,2,256]{0,2,1:T(8,128)(2,1)} %bitcast.145), calls=%async_computation | async-start | bytes 2097152 | tf_op jit(solution)/shard_map/all_to_all | solution.py:175
  100.5 16.2 %all-to-all-start.2 = ((bf16[1024,2,256]{0,2,1:T(8,128)(2,1)}), bf16[1024,2,256]{0,2,1:T(8,128)(2,1)}, u32[]{:S(2)}, u32[]{:S(2)}) async-start(bf16[1024,2,256]{0,2,1:T(8,128)(2,1)} %bitcast.146), calls=%async_computation.2 | async-start | bytes 2097152 | tf_op jit(solution)/shard_map/all_to_all | solution.py:176
  107.3 14.6 %copy-start.11 = (f32[4]{0:T(128)S(1)}, f32[4]{0:T(128)}, u32[]{:S(2)}) copy-start(f32[4]{0:T(128)} %param.29) | copy-start | bytes 52
  116.7 15.3 %all-to-all-start.1 = ((bf16[1024,2,256]{0,2,1:T(8,128)(2,1)}), bf16[1024,2,256]{0,2,1:T(8,128)(2,1)}, u32[]{:S(2)}, u32[]{:S(2)}) async-start(bf16[1024,2,256]{0,2,1:T(8,128)(2,1)} %bitcast.141), calls=%async_computation.1 | async-start | bytes 2097152 | tf_op jit(solution)/shard_map/all_to_all | solution.py:174
  121.1 133.7 %all-gather.9.cloned.1.call-start = ((), (), s32[]{:S(2)}) async-start(), calls=%async_computation.10 | async-start | bytes 3145728 | tf_op jit(solution)/shard_map/all_gather | solution.py:219
  128.3 5.3 %copy-start.7 = (bf16[2,1024,256]{2,1,0:T(8,128)(2,1)S(1)}, bf16[2,1024,256]{2,1,0:T(8,128)(2,1)}, u32[]{:S(2)}) copy-start(bf16[2,1024,256]{2,1,0:T(8,128)(2,1)} %copy.93) | copy-start | bytes 3145732
  133.6 6.3 %copy-start.1 = (bf16[1,256,2048]{2,1,0:T(8,128)(2,1)S(1)}, bf16[1,256,2048]{2,1,0:T(8,128)(2,1)}, u32[]{:S(2)}) copy-start(bf16[1,256,2048]{2,1,0:T(8,128)(2,1)} %all-gather.11.cloned.1.call-done) | copy-start | bytes 3145732
  138.0 7.8 %copy-start.3 = (bf16[2,1024,256]{2,1,0:T(8,128)(2,1)S(1)}, bf16[2,1024,256]{2,1,0:T(8,128)(2,1)}, u32[]{:S(2)}) copy-start(bf16[2,1024,256]{2,1,0:T(8,128)(2,1)} %copy.96) | copy-start | bytes 3145732
  174.6 23.2 %copy-start.2 = (bf16[2,1024,256]{2,1,0:T(8,128)(2,1)S(1)}, bf16[2,1024,256]{2,1,0:T(8,128)(2,1)}, u32[]{:S(2)}) copy-start(bf16[2,1024,256]{2,1,0:T(8,128)(2,1)} %copy.88) | copy-start | bytes 3145732
  239.1 7.6 %copy-start.8 = (f32[2,128,2,128]{1,3,2,0:T(8,128)S(1)}, f32[2,128,2,128]{1,3,2,0:T(8,128)}, u32[]{:S(2)}) copy-start(f32[2,128,2,128]{1,3,2,0:T(8,128)} %copy.104) | copy-start | bytes 786436
  239.1 7.6 %copy-start.9 = (f32[2,128,2,128]{3,2,1,0:T(2,128)S(1)}, f32[2,128,2,128]{3,2,1,0:T(2,128)}, u32[]{:S(2)}) copy-start(f32[2,128,2,128]{3,2,1,0:T(2,128)} %get-tuple-element.520) | copy-start | bytes 786436
  239.9 8.3 %all-to-all-start.3 = ((bf16[2,128,256]{1,2,0:T(8,128)(2,1)}), bf16[2,128,256]{1,2,0:T(8,128)(2,1)S(1)}, u32[]{:S(2)}, u32[]{:S(2)}) async-start(bf16[2,128,256]{1,2,0:T(8,128)(2,1)} %bitcast.17), calls=%async_computation.3 | async-start | bytes 262144 | tf_op jit(solution)/shard_map/all_to_all | solution.py:214
  243.3 4.1 %copy-start.10 = (f32[128]{0:T(128)S(1)}, f32[128]{0:T(128)}, u32[]{:S(2)}) copy-start(f32[128]{0:T(128)} %param.31) | copy-start | bytes 1540
  248.2 6.7 %all-to-all-start.7 = ((bf16[2,128,256]{1,2,0:T(8,128)(2,1)}), bf16[2,128,256]{1,2,0:T(8,128)(2,1)S(1)}, u32[]{:S(2)}, u32[]{:S(2)}) async-start(bf16[2,128,256]{1,2,0:T(8,128)(2,1)} %bitcast.38), calls=%async_computation.7 | async-start | bytes 262144 | tf_op jit(solution)/shard_map/all_to_all | solution.py:215
  251.5 26.5 %reduce-scatter.2.cloned.1.call-start = ((), (), s32[]{:S(2)}) async-start(), calls=%async_computation.11 | async-start | bytes 786432 | tf_op jit(solution)/shard_map/reduce_scatter | solution.py:222
Sparse Core Ops, SparseCore 0:
  11.4 30.2 all-gather.10
  43.2 49.8 all-gather.6
  123.5 36.5 all-gather.8
  257.9 20.0 reduce-scatter.1
where the time goes:
time: 287 us; the launch traced here: 285 us
  waiting for transfers between devices  98.4 us (34%)
  blocking collectives  50.9 us (18%)
  local copies, waits for them, and re-layouts  35.2 us (12%)
  starting transfers between devices  31 us (11%)
  other arithmetic  28.7 us (10%)
  matrix products  26.3 us (9%)
  between operations  13.5 us (5%)
    all_to_all x1, waiting for transfers between devices, body(): lax.all_to_all(weights[5], 'fs', split_axis=1, concat_axis=0, tiled=True)  21.6 us
    all_gather x2, blocking collectives, carried_in(): lax.all_gather(a.astype(kind), axis)  20.4 us
    reduce_scatter x1, waiting for transfers between devices, body(): lax.psum_scatter((jnp.dot(attn_flat, full_attn, preferred_element_type=jn...  20.3 us
    all_to_all x1, waiting for transfers between devices, body(): lax.all_to_all(weights[4], 'fs', split_axis=1, concat_axis=0, tiled=True)  19.4 us
    another operation x4, other arithmetic, compute(): inner_sum = lax.cumsum(log_keep, axis=3, reverse=True) - log_keep  17.7 us
    all_to_all x1, waiting for transfers between devices, body(): lax.all_to_all(weights[1], 'fs', split_axis=1, concat_axis=0, tiled=True)  14.9 us
    all_gather x1, blocking collectives, stick_mixer(): value_all = lax.all_gather(value_rows, 'sp', axis=1, tiled=True)  13.9 us
    all_gather x1, blocking collectives, stick_mixer(): key_all = lax.all_gather(key_rows, 'sp', axis=1, tiled=True)  13.9 us
  transfers between devices with their start and end apart: 12, of which 8 were waited for; matrix products, arithmetic and copies ran while one was open for 30% of the time, Pallas kernels for 0%

commit v1 on v0

v1 whole, which is shorter than its diff:
```python
import functools
import math

import jax
import jax.numpy as jnp
from jax import lax
from jax.experimental import pallas as pl
from jax.experimental.pallas import tpu as pltpu
from jax.sharding import PartitionSpec as P

LANES = 128
norm_eps = 1e-06
MESH = pl.DeviceIdType.MESH
F32 = jnp.float32
BF16 = jnp.bfloat16
N_PROJ = 6


def dot_nn(a, b):
    return lax.dot_general(a, b, (((1,), (0,)), ((), ())), preferred_element_type=F32)


def dot_nt(a, b):
    return lax.dot_general(a, b, (((1,), (1,)), ((), ())), preferred_element_type=F32)


def dot_tn(a, b):
    return lax.dot_general(a, b, (((0,), (0,)), ((), ())), preferred_element_type=F32)


def halves(x):
    high = x.astype(BF16)
    return high, (x - high.astype(F32)).astype(BF16)


def kernel(
    n_sp, n_fs, n_tp,
    tok, gain, w_k, w_v, w_f, w_i, w_q, w_r, offs, room, out_gain, o_attn, o_rec,
    out,
    wbuf, obuf, xt, xg, ss, acc, psend, precv, kv, qbuf, qdec, ecum, kinv,
    att, run, loc, st_loc, dec, st_in, st_out, heads, hrecv, part, precv2, mix, mrecv,
    w_sem, x_send, x_recv, ss_send, ss_recv, p_send, p_recv, kv_send, kv_recv,
    st_sem, h_send, h_recv, pp_send, pp_recv, m_send, m_recv,
):
    sp, fs, tp = lax.axis_index("sp"), lax.axis_index("fs"), lax.axis_index("tp")
    rows, feat_t = tok.shape
    feat_f = xt.shape[2]
    width = feat_t * n_tp
    cols = wbuf.shape[2]
    n_heads = cols // LANES
    share = rows // n_tp
    out_cols = obuf.shape[2]
    has_next = sp < n_sp - 1
    has_prev = sp > 0

    def fs_at(step):
        return lax.rem(fs + step, n_fs)

    def tp_at(step):
        return lax.rem(tp + step, n_tp)

    w_copies = [
        pltpu.make_async_copy(w, wbuf.at[i], w_sem.at[i])
        for i, w in enumerate((w_k, w_v, w_f, w_i, w_q, w_r))
    ]
    w_copies += [
        pltpu.make_async_copy(w, obuf.at[i], w_sem.at[N_PROJ + i])
        for i, w in enumerate((o_attn, o_rec))
    ]
    for copy in w_copies:
        copy.start()

    barrier = pltpu.get_barrier_semaphore()
    for df in range(n_fs):
        for dt in range(n_tp):
            if df or dt:
                pl.semaphore_signal(
                    barrier, inc=1, device_id={"fs": fs_at(df), "tp": tp_at(dt)}, device_id_type=MESH
                )

    @pl.when(has_next)
    def _():
        pl.semaphore_signal(barrier, inc=1, device_id={"sp": sp + 1}, device_id_type=MESH)

    @pl.when(has_prev)
    def _():
        pl.semaphore_signal(barrier, inc=1, device_id={"sp": sp - 1}, device_id_type=MESH)

    squares = jnp.zeros((rows, LANES), F32)
    for c in range(feat_t // LANES):
        piece = tok[:, c * LANES:(c + 1) * LANES].astype(F32)
        squares = squares + piece * piece
    ss[tp] = squares

    next_count = jnp.where(has_next, 1, 0)
    prev_count = jnp.where(has_prev, 1, 0)
    pl.semaphore_wait(barrier, n_fs * n_tp - 1 + next_count + prev_count)

    def holder(f_index):
        return (f_index * feat_f) // feat_t

    def x_copy(df, dt):
        dest = fs_at(df)
        start = pl.multiple_of(lax.rem(dest * feat_f, feat_t), LANES)
        return pltpu.make_async_remote_copy(
            src_ref=tok.at[:, pl.ds(start, feat_f)],
            dst_ref=xt.at[fs],
            send_sem=x_send.at[df * n_tp + dt],
            recv_sem=x_recv.at[fs],
            device_id={"fs": dest, "tp": tp_at(dt)},
            device_id_type=MESH,
        )

    x_order = [(df, dt) for df in list(range(1, n_fs)) + [0] for dt in range(n_tp) if df or dt]
    for df, dt in x_order:
        @pl.when(holder(fs_at(df)) == tp)
        def _(df=df, dt=dt):
            x_copy(df, dt).start()

    def ss_copy(dt):
        return pltpu.make_async_remote_copy(
            src_ref=ss.at[tp], dst_ref=ss.at[tp],
            send_sem=ss_send.at[dt - 1], recv_sem=ss_recv.at[tp],
            device_id={"tp": tp_at(dt)}, device_id_type=MESH,
        )

    for dt in range(1, n_tp):
        ss_copy(dt).start()

    own_holder = holder(fs) == tp
    gain_f = gain[:, pl.ds(pl.multiple_of(fs * feat_f, LANES), feat_f)]

    @pl.when(own_holder)
    def _():
        start = pl.multiple_of(lax.rem(fs * feat_f, feat_t), LANES)
        xg[0] = (tok[:, pl.ds(start, feat_f)].astype(F32) * gain_f).astype(BF16)

    def x_wait(slot):
        pltpu.make_async_remote_copy(
            src_ref=xt.at[slot], dst_ref=xt.at[slot],
            send_sem=x_send.at[0], recv_sem=x_recv.at[slot],
            device_id={"tp": tp_at(1)}, device_id_type=MESH,
        ).wait_recv()

    def p_copy(df, w):
        return pltpu.make_async_remote_copy(
            src_ref=psend.at[df - 1, w], dst_ref=precv.at[df - 1, w],
            send_sem=p_send.at[(df - 1) * N_PROJ + w], recv_sem=p_recv.at[(df - 1) * N_PROJ + w],
            device_id={"fs": fs_at(df)}, device_id_type=MESH,
        )

    for df in range(1, n_fs):
        slot = fs_at(df)
        x_wait(slot)
        xg[df] = (xt[slot].astype(F32) * gain_f).astype(BF16)
    for w in range(N_PROJ):
        w_copies[w].wait()
        for df in range(1, n_fs):
            psend[df - 1, w] = dot_nn(xg[df], wbuf[w]).astype(BF16)
            p_copy(df, w).start()

    @pl.when(jnp.logical_not(own_holder))
    def _():
        x_wait(fs)
        xg[0] = (xt[fs].astype(F32) * gain_f).astype(BF16)

    for w in range(N_PROJ):
        acc[w] = dot_nn(xg[0], wbuf[w])

    total = ss[tp]
    for dt in range(1, n_tp):
        other = tp_at(dt)
        pltpu.make_async_remote_copy(
            src_ref=ss.at[other], dst_ref=ss.at[other],
            send_sem=ss_send.at[dt - 1], recv_sem=ss_recv.at[other],
            device_id={"tp": other}, device_id_type=MESH,
        ).wait_recv()
        total = total + ss[other]
    factor = lax.rsqrt(jnp.sum(total, axis=1, keepdims=True) / width + norm_eps)

    def finish(w):
        value = acc[w]
        for df in range(1, n_fs):
            p_copy(df, w).wait_recv()
            value = value + precv[df - 1, w].astype(F32)
        return (value * factor).astype(BF16)

    def kv_copy(slot, c):
        return pltpu.make_async_remote_copy(
            src_ref=kv.at[slot, c], dst_ref=kv.at[slot, c],
            send_sem=kv_send.at[slot * 2 + c], recv_sem=kv_recv.at[slot * 2 + c],
            device_id={"sp": lax.rem(sp + 1, n_sp)}, device_id_type=MESH,
        )

    for c in range(2):
        kv[sp, c] = finish(c)

        @pl.when(has_next)
        def _(c=c):
            kv_copy(sp, c).start()

    iota_r = lax.broadcasted_iota(jnp.int32, (rows, rows), 0)
    iota_c = lax.broadcasted_iota(jnp.int32, (rows, rows), 1)
    causal = iota_r >= iota_c
    strict = iota_c < iota_r

    def st_copy():
        return pltpu.make_async_remote_copy(
            src_ref=st_out, dst_ref=st_in, send_sem=st_sem.at[0], recv_sem=st_sem.at[1],
            device_id={"sp": lax.rem(sp + 1, n_sp)}, device_id_type=MESH,
        )

    lower = jnp.where(causal, 1.0, 0.0).astype(BF16)
    forget_pre = finish(2)
    rec_i = finish(3)
    for h in range(n_heads):
        lanes = slice(h * LANES, (h + 1) * LANES)
        key_in = room[h:h + 1, :] * jax.nn.sigmoid(-forget_pre[:, lanes].astype(F32))
        high, low = halves(jnp.log1p(-key_in))
        cum = dot_nn(lower, high) + dot_nn(lower, low)
        last = cum[rows - 1:rows, :]
        ecum[:, lanes] = jnp.exp(cum)
        kinv[:, lanes] = (key_in * jnp.exp(-cum)).astype(BF16)
        fresh = (key_in * jnp.exp(last - cum)).astype(BF16)
        st_loc[h] = dot_tn(rec_i[:, lanes], fresh)
        dec[h] = jnp.broadcast_to(jnp.exp(last), dec.shape[1:])

    @pl.when(jnp.logical_and(sp == 0, has_next))
    def _():
        st_out[...] = st_loc[...].astype(BF16)
        st_copy().start()

    qbuf[...] = finish(4)
    later = jnp.where(iota_r > iota_c, 1.0, 0.0).astype(BF16)
    sums = jnp.concatenate([later, jnp.ones((rows, LANES), BF16)], axis=1)
    scale = 1.0 / math.sqrt(LANES)

    def attend(slot, diagonal):
        for h in range(n_heads):
            lanes = slice(h * LANES, (h + 1) * LANES)
            z = dot_nt(qbuf[:, lanes], kv[slot, 0, :, lanes]) * scale + offs[h]
            keep = -(jnp.maximum(z, 0.0) + jnp.log1p(jnp.exp(-jnp.abs(z))))
            log_stick = z + keep
            if diagonal:
                keep = jnp.where(strict, keep, 0.0)
            high, low = halves(keep)
            both = dot_nn(high, sums) + dot_nn(low, sums)
            stick = jnp.exp(log_stick + both[:, :rows])
            if diagonal:
                stick = jnp.where(strict, stick, 0.0)
            value = dot_nn(stick.astype(BF16), kv[slot, 1, :, lanes])
            if diagonal:
                att[:, lanes] = value
                run[h] = both[:, rows:]
            else:
                past = run[h]
                att[:, lanes] += value * jnp.exp(past)
                run[h] = past + both[:, rows:]

    attend(sp, True)

    rec_q = finish(5)
    for h in range(n_heads):
        lanes = slice(h * LANES, (h + 1) * LANES)
        decayed = (rec_q[:, lanes].astype(F32) * ecum[:, lanes]).astype(BF16)
        qdec[:, lanes] = decayed
        scores = jnp.where(causal, dot_nt(decayed, kinv[:, lanes]), 0.0)
        loc[:, lanes] = dot_nn(scores.astype(BF16), rec_i[:, lanes])

    def block(step, carry):
        slot = sp - step
        for c in range(2):
            kv_copy(slot, c).wait_recv()

            @pl.when(has_next)
            def _(c=c):
                kv_copy(slot, c).start()
        attend(slot, False)
        return carry

    lax.fori_loop(1, sp + 1, block, 0)

    def h_copy(df, c):
        return pltpu.make_async_remote_copy(
            src_ref=heads.at[c], dst_ref=hrecv.at[df - 1, c],
            send_sem=h_send.at[(df - 1) * 2 + c], recv_sem=h_recv.at[(df - 1) * 2 + c],
            device_id={"fs": fs_at(df)}, device_id_type=MESH,
        )

    heads[0] = att[...].astype(BF16)
    for df in range(1, n_fs):
        h_copy(df, 0).start()

    @pl.when(has_prev)
    def _():
        st_copy().wait_recv()

        @pl.when(has_next)
        def _():
            for h in range(n_heads):
                st_out[h] = (st_in[h].astype(F32) * dec[h, 0:1, :] + st_loc[h]).astype(BF16)
            st_copy().start()

        for h in range(n_heads):
            lanes = slice(h * LANES, (h + 1) * LANES)
            loc[:, lanes] += dot_nt(qdec[:, lanes], st_in[h])

    for h in range(n_heads):
        lanes = slice(h * LANES, (h + 1) * LANES)
        raw = loc[:, lanes]
        norm = lax.rsqrt(jnp.mean(raw * raw, axis=1, keepdims=True) + norm_eps)
        heads[1, :, lanes] = (raw * norm * out_gain[...]).astype(BF16)
    for df in range(1, n_fs):
        h_copy(df, 1).start()

    w_copies[N_PROJ].wait()
    w_copies[N_PROJ + 1].wait()

    def pp_copy(df, dt):
        index = df * (n_tp - 1) + dt - 1
        start = pl.multiple_of(tp_at(dt) * share, share)
        return pltpu.make_async_remote_copy(
            src_ref=part.at[df, pl.ds(start, share)], dst_ref=precv2.at[dt - 1, df],
            send_sem=pp_send.at[index], recv_sem=pp_recv.at[index],
            device_id={"tp": tp_at(dt)}, device_id_type=MESH,
        )

    def m_copy(df):
        return pltpu.make_async_remote_copy(
            src_ref=mix.at[df - 1], dst_ref=mrecv.at[df - 1],
            send_sem=m_send.at[df - 1], recv_sem=m_recv.at[df - 1],
            device_id={"fs": fs_at(df)}, device_id_type=MESH,
        )

    def project(df, first, second):
        part[df] = (dot_nn(first, obuf[0]) + dot_nn(second, obuf[1])).astype(BF16)
        for dt in range(1, n_tp):
            pp_copy(df, dt).start()

    def reduced(df):
        value = part[df, pl.ds(pl.multiple_of(tp * share, share), share)].astype(F32)
        for dt in range(1, n_tp):
            pp_copy(df, dt).wait_recv()
            value = value + precv2[dt - 1, df].astype(F32)
        return value.astype(BF16)

    project(0, heads[0], heads[1])
    for df in range(1, n_fs):
        h_copy(df, 0).wait_recv()
        h_copy(df, 1).wait_recv()
        project(df, hrecv[df - 1, 0], hrecv[df - 1, 1])
    for df in range(1, n_fs):
        mix[df - 1] = reduced(df)
        m_copy(df).start()
    out[:, pl.ds(pl.multiple_of(fs * out_cols, LANES), out_cols)] = reduced(0)
    for df in range(1, n_fs):
        m_copy(df).wait_recv()
        source = lax.rem(fs + n_fs - df, n_fs)
        out[:, pl.ds(pl.multiple_of(source * out_cols, LANES), out_cols)] = mrecv[df - 1]

    for df, dt in x_order:
        @pl.when(holder(fs_at(df)) == tp)
        def _(df=df, dt=dt):
            x_copy(df, dt).wait_send()
    for dt in range(1, n_tp):
        ss_copy(dt).wait_send()
    for df in range(1, n_fs):
        for w in range(N_PROJ):
            p_copy(df, w).wait_send()
        for c in range(2):
            h_copy(df, c).wait_send()
        m_copy(df).wait_send()
    for df in range(n_fs):
        for dt in range(1, n_tp):
            pp_copy(df, dt).wait_send()

    @pl.when(has_next)
    def _():
        st_copy().wait_send()

        def drain(slot, carry):
            for c in range(2):
                kv_copy(slot, c).wait_send()
            return carry

        lax.fori_loop(0, sp + 1, drain, 0)


def body(
    tokens, mix_gain, attn_query, attn_key, attn_value, rec_query, rec_forget, rec_input,
    break_offset, forget_room, out_gain, out_attn, out_rec,
):
    n_sp, n_fs, n_tp = lax.axis_size("sp"), lax.axis_size("fs"), lax.axis_size("tp")
    rows, feat_t = tokens.shape[1], tokens.shape[2]
    feat_f, cols = attn_query.shape
    width = feat_t * n_tp
    n_heads = cols // LANES
    out_rows, out_cols = out_attn.shape
    share = rows // n_tp
    vmem = pl.BlockSpec(memory_space=pltpu.VMEM)
    smem = pl.BlockSpec(memory_space=pltpu.SMEM)
    hbm = pl.BlockSpec(memory_space=pl.ANY)
    dma = pltpu.SemaphoreType.DMA
    square = (n_heads, LANES, LANES)
    result = pl.pallas_call(
        functools.partial(kernel, n_sp, n_fs, n_tp),
        out_shape=jax.ShapeDtypeStruct((share, width), BF16),
        in_specs=[vmem, vmem] + [hbm] * 6 + [smem, vmem, vmem, hbm, hbm],
        out_specs=vmem,
        scratch_shapes=[
            pltpu.VMEM((N_PROJ, feat_f, cols), BF16),
            pltpu.VMEM((2, out_rows, out_cols), BF16),
            pltpu.VMEM((n_fs, rows, feat_f), BF16),
            pltpu.VMEM((n_fs, rows, feat_f), BF16),
            pltpu.VMEM((n_tp, rows, LANES), F32),
            pltpu.VMEM((N_PROJ, rows, cols), F32),
            pltpu.VMEM((n_fs - 1, N_PROJ, rows, cols), BF16),
            pltpu.VMEM((n_fs - 1, N_PROJ, rows, cols), BF16),
            pltpu.VMEM((n_sp, 2, rows, cols), BF16),
            pltpu.VMEM((rows, cols), BF16),
            pltpu.VMEM((rows, cols), BF16),
            pltpu.VMEM((rows, cols), F32),
            pltpu.VMEM((rows, cols), BF16),
            pltpu.VMEM((rows, cols), F32),
            pltpu.VMEM((n_heads, rows, LANES), F32),
            pltpu.VMEM((rows, cols), F32),
            pltpu.VMEM(square, F32),
            pltpu.VMEM((n_heads, 8, LANES), F32),
            pltpu.VMEM(square, BF16),
            pltpu.VMEM(square, BF16),
            pltpu.VMEM((2, rows, cols), BF16),
            pltpu.VMEM((n_fs - 1, 2, rows, cols), BF16),
            pltpu.VMEM((n_fs, rows, out_cols), BF16),
            pltpu.VMEM((n_tp - 1, n_fs, share, out_cols), BF16),
            pltpu.VMEM((n_fs - 1, share, out_cols), BF16),
            pltpu.VMEM((n_fs - 1, share, out_cols), BF16),
            dma((N_PROJ + 2,)),
            dma((n_fs * n_tp,)), dma((n_fs,)),
            dma((n_tp - 1,)), dma((n_tp,)),
            dma(((n_fs - 1) * N_PROJ,)), dma(((n_fs - 1) * N_PROJ,)),
            dma((n_sp * 2,)), dma((n_sp * 2,)),
            dma((2,)),
            dma(((n_fs - 1) * 2,)), dma(((n_fs - 1) * 2,)),
            dma((n_fs * (n_tp - 1),)), dma((n_fs * (n_tp - 1),)),
            dma((n_fs - 1,)), dma((n_fs - 1,)),
        ],
        compiler_params=pltpu.CompilerParams(
            collective_id=0, has_side_effects=True, vmem_limit_bytes=60 * 1024 * 1024
        ),
        name="layer",
    )(
        tokens.reshape(rows, feat_t), mix_gain.reshape(1, width),
        attn_key, attn_value, rec_forget, rec_input, attn_query, rec_query,
        break_offset, forget_room, out_gain.reshape(1, LANES), out_attn, out_rec,
    )
    return result.reshape(1, share, width)


def solution(mesh):
    placed = (
        P(("grp", "fs"), "sp", "tp"),
        P(),
        P("fs", "tp"),
        P("fs", "tp"),
        P("fs", "tp"),
        P("fs", "tp"),
        P("fs", "tp"),
        P("fs", "tp"),
        P("tp"),
        P("tp", None),
        P(),
        P("tp", "fs"),
        P("tp", "fs"),
    )
    return jax.shard_map(
        body,
        mesh=mesh,
        in_specs=placed,
        out_specs=P(("grp", "fs"), ("sp", "tp"), None),
        check_vma=False,
    )
```

time: 287 us -> 56.5 us (0.20)
  waiting for transfers between devices: 98.4 us -> 0 us
  Pallas kernels: 0 us -> 54.7 us
  blocking collectives: 50.9 us -> 0 us
  local copies, waits for them, and re-layouts: 35.2 us -> 1.67 us
  starting transfers between devices: 31 us -> 0 us
  other arithmetic: 28.7 us -> 0 us
  matrix products: 26.3 us -> 0 us
  between operations: 13.5 us -> 0.01 us
    all_to_all x8 -> x0, waiting for transfers between devices: 76.7 us -> none  [the longest x1 21.6 us: body(): lax.all_to_all(weights[5], 'fs', split_axis=1, concat_axis=0, tiled=True)]
    pallas_call x0 -> x1, Pallas kernels: none -> 54.7 us  [body(): pl.pallas_call(functools.partial(kernel, n_sp, n_fs, n_tp), out_shape=jax...]
    all_gather x5 -> x0, blocking collectives: 50.9 us -> none  [the longest x2 20.4 us: carried_in(): lax.all_gather(a.astype(kind), axis)]
    all_to_all x8 -> x0, starting transfers between devices: 30.8 us -> none  [the longest x1 4.48 us: body(): lax.all_to_all(weights[2], 'fs', split_axis=1, concat_axis=0, tiled=True)]
    dot_general x25 -> x0, matrix products: 26.3 us -> none  [the longest x6 8.68 us: body(): jnp.dot(pieces, matrix, preferred_element_type=jnp.float32)]
    another operation x8 -> x0, other arithmetic: 20.3 us -> none  [the longest x4 17.7 us: compute(): inner_sum = lax.cumsum(log_keep, axis=3, reverse=True) - log_keep]
    reduce_scatter x1 -> x0, waiting for transfers between devices: 20.3 us -> none  [body(): lax.psum_scatter((jnp.dot(attn_flat, full_attn, preferred_element_type=jn...]
    all_to_all x6 -> x0, local copies, waits for them, and re-layouts: 10.1 us -> none  [the longest x1 2.36 us: body(): lax.all_to_all(weights[2], 'fs', split_axis=1, concat_axis=0, tiled=True)]
  transfers between devices with their start and end apart: 12 -> 0, of which waited for: 8 -> 0; matrix products, arithmetic and copies ran while one was open for 30% -> 0% of each run, Pallas kernels for 0% -> 0%
where the time goes in v1:
time: 56.5 us; the launch traced here: 56.4 us
  Pallas kernels  54.7 us (97%)
  local copies, waits for them, and re-layouts  1.67 us (3%)
    pallas_call x1, Pallas kernels, body(): pl.pallas_call(functools.partial(kernel, n_sp, n_fs, n_tp), out_shape=jax...  54.7 us
    unnamed x1, local copies, waits for them, and re-layouts  1.67 us

profile of v1, /device:TPU:29, one launch (start us, length us, event | category | flops | bytes accessed | tf_op | source)
XLA Modules:
  0.0 56.4 jit_solution(2655574648424165122)
XLA Ops:
  0.0 54.7 %layer.1 = bf16[64,2048]{1,0:T(8,128)(2,1)} custom-call(bf16[128,1024]{1,0:T(8,128)(2,1)} %bitcast.5, f32[1,2048]{1,0:T(1,128)} %bitcast.6, bf16[1024,512]{1,0:T(8,128)(2,1)} %w_k.1, bf16[1024,512]{1,0:T(8,128)(2,1)} %w_v.1, bf16[1024,512]{1,0:T(8,128)(2,1)} %w_f.1, bf16[1024,512]{1,0:T(8,128)(2,1)} %w_i.1, bf16[1024,512]{1,0:T(8,128)(2,1)} %w_q.1, ...), custom_call_target="tpu_custom_call" | custom-call | tf_op jit(solution)/shard_map/layer/pallas_call | solution.py:405
  54.7 1.7 %copy.15 = bf16[1,64,2048]{2,1,0:T(8,128)(2,1)} copy(bf16[1,64,2048]{2,1,0:T(8,128)(2,1)} %bitcast.4) | data formatting | bytes 524288

commit v2 on v1

--- a/solution.py
+++ b/solution.py
@@ -14,6 +14,7 @@
 F32 = jnp.float32
 BF16 = jnp.bfloat16
 N_PROJ = 6
+CHUNKS = 2
 
 
 def dot_nn(a, b):
@@ -35,11 +36,11 @@
 
 def kernel(
     n_sp, n_fs, n_tp,
-    tok, gain, w_k, w_v, w_f, w_i, w_q, w_r, offs, room, out_gain, o_attn, o_rec,
+    tok_hbm, gain, w_k, w_v, w_f, w_i, w_q, w_r, offs, room, out_gain, o_attn, o_rec,
     out,
-    wbuf, obuf, xt, xg, ss, acc, psend, precv, kv, qbuf, qdec, ecum, kinv,
-    att, run, loc, st_loc, dec, st_in, st_out, heads, hrecv, part, precv2, mix, mrecv,
-    w_sem, x_send, x_recv, ss_send, ss_recv, p_send, p_recv, kv_send, kv_recv,
+    tok, wbuf, obuf, xt, xg, ss, acc, psend, precv, kv, qbuf, qdec, ecum, kinv,
+    att, run, loc, st_loc, dec, st_in, st_out, heads, hrecv, part_acc, part, precv2, mix, mrecv,
+    t_sem, w_sem, x_send, x_recv, f_send, ss_send, ss_recv, p_send, p_recv, kv_send, kv_recv,
     st_sem, h_send, h_recv, pp_send, pp_recv, m_send, m_recv,
 ):
     sp, fs, tp = lax.axis_index("sp"), lax.axis_index("fs"), lax.axis_index("tp")
@@ -59,6 +60,8 @@
     def tp_at(step):
         return lax.rem(tp + step, n_tp)
 
+    tok_copy = pltpu.make_async_copy(tok_hbm, tok, t_sem.at[0])
+    tok_copy.start()
     w_copies = [
         pltpu.make_async_copy(w, wbuf.at[i], w_sem.at[i])
         for i, w in enumerate((w_k, w_v, w_f, w_i, w_q, w_r))
@@ -67,9 +70,6 @@
         pltpu.make_async_copy(w, obuf.at[i], w_sem.at[N_PROJ + i])
         for i, w in enumerate((o_attn, o_rec))
     ]
-    for copy in w_copies:
-        copy.start()
-
     barrier = pltpu.get_barrier_semaphore()
     for df in range(n_fs):
         for dt in range(n_tp):
@@ -86,37 +86,56 @@
     def _():
         pl.semaphore_signal(barrier, inc=1, device_id={"sp": sp - 1}, device_id_type=MESH)
 
+    for copy in w_copies:
+        copy.start()
+    tok_copy.wait()
+
+    next_count = jnp.where(has_next, 1, 0)
+    prev_count = jnp.where(has_prev, 1, 0)
+    pl.semaphore_wait(barrier, n_fs * n_tp - 1 + next_count + prev_count)
+
+    def holder(f_index):
+        return (f_index * feat_f) // feat_t
+
+    def x_copy(df, dt):
+        dest = fs_at(df)
+        start = pl.multiple_of(lax.rem(dest * feat_f, feat_t), LANES)
+        part_rows = rows if df == 0 else share
+        first = 0 if df == 0 else pl.multiple_of(tp_at(dt) * share, share)
+        piece = tp if df == 0 else tp_at(dt)
+        return pltpu.make_async_remote_copy(
+            src_ref=tok.at[pl.ds(first, part_rows), pl.ds(start, feat_f)],
+            dst_ref=xt.at[fs, pl.ds(first, part_rows)],
+            send_sem=x_send.at[df * n_tp + dt],
+            recv_sem=x_recv.at[fs * n_tp + piece],
+            device_id={"fs": dest, "tp": tp_at(dt)},
+            device_id_type=MESH,
+        )
+
+    def f_copy(df, dt):
+        slot = fs_at(df)
+        first = pl.multiple_of(tp * share, share)
+        return pltpu.make_async_remote_copy(
+            src_ref=xt.at[slot, pl.ds(first, share)],
+            dst_ref=xt.at[slot, pl.ds(first, share)],
+            send_sem=f_send.at[df * n_tp + dt],
+            recv_sem=x_recv.at[slot * n_tp + tp],
+            device_id={"tp": tp_at(dt)},
+            device_id_type=MESH,
+        )
+
+    x_order = [(df, dt) for df in list(range(1, n_fs)) + [0] for dt in range(n_tp) if df or dt]
+    for df, dt in x_order:
+        @pl.when(holder(fs_at(df)) == tp)
+        def _(df=df, dt=dt):
+            x_copy(df, dt).start()
+
     squares = jnp.zeros((rows, LANES), F32)
     for c in range(feat_t // LANES):
         piece = tok[:, c * LANES:(c + 1) * LANES].astype(F32)
         squares = squares + piece * piece
     ss[tp] = squares
 
-    next_count = jnp.where(has_next, 1, 0)
-    prev_count = jnp.where(has_prev, 1, 0)
-    pl.semaphore_wait(barrier, n_fs * n_tp - 1 + next_count + prev_count)
-
-    def holder(f_index):
-        return (f_index * feat_f) // feat_t
-
-    def x_copy(df, dt):
-        dest = fs_at(df)
-        start = pl.multiple_of(lax.rem(dest * feat_f, feat_t), LANES)
-        return pltpu.make_async_remote_copy(
-            src_ref=tok.at[:, pl.ds(start, feat_f)],
-            dst_ref=xt.at[fs],
-            send_sem=x_send.at[df * n_tp + dt],
-            recv_sem=x_recv.at[fs],
-            device_id={"fs": dest, "tp": tp_at(dt)},
-            device_id_type=MESH,
-        )
-
-    x_order = [(df, dt) for df in list(range(1, n_fs)) + [0] for dt in range(n_tp) if df or dt]
-    for df, dt in x_order:
-        @pl.when(holder(fs_at(df)) == tp)
-        def _(df=df, dt=dt):
-            x_copy(df, dt).start()
-
     def ss_copy(dt):
         return pltpu.make_async_remote_copy(
             src_ref=ss.at[tp], dst_ref=ss.at[tp],
@@ -135,10 +154,11 @@
         start = pl.multiple_of(lax.rem(fs * feat_f, feat_t), LANES)
         xg[0] = (tok[:, pl.ds(start, feat_f)].astype(F32) * gain_f).astype(BF16)
 
-    def x_wait(slot):
+    def x_wait(slot, piece, first, count):
+        view = xt.at[slot, pl.ds(first, count)]
         pltpu.make_async_remote_copy(
-            src_ref=xt.at[slot], dst_ref=xt.at[slot],
-            send_sem=x_send.at[0], recv_sem=x_recv.at[slot],
+            src_ref=view, dst_ref=view,
+            send_sem=x_send.at[0], recv_sem=x_recv.at[slot * n_tp + piece],
             device_id={"tp": tp_at(1)}, device_id_type=MESH,
         ).wait_recv()
 
@@ -151,7 +171,14 @@
 
     for df in range(1, n_fs):
         slot = fs_at(df)
-        x_wait(slot)
+        x_wait(slot, tp, pl.multiple_of(tp * share, share), share)
+        for dt in range(1, n_tp):
+            f_copy(df, dt).start()
+    for df in range(1, n_fs):
+        slot = fs_at(df)
+        for dt in range(1, n_tp):
+            piece = tp_at(dt)
+            x_wait(slot, piece, pl.multiple_of(piece * share, share), share)
         xg[df] = (xt[slot].astype(F32) * gain_f).astype(BF16)
     for w in range(N_PROJ):
         w_copies[w].wait()
@@ -161,7 +188,7 @@
 
     @pl.when(jnp.logical_not(own_holder))
     def _():
-        x_wait(fs)
+        x_wait(fs, holder(fs), 0, rows)
         xg[0] = (xt[fs].astype(F32) * gain_f).astype(BF16)
 
     for w in range(N_PROJ):
@@ -199,19 +226,33 @@
         def _(c=c):
             kv_copy(sp, c).start()
 
+    def hand_on(step, c):
+        kv_copy(sp - step, c).wait_recv()
+
+        @pl.when(has_next)
+        def _():
+            kv_copy(sp - step, c).start()
+
+    def hand_on_if(step, c):
+        if step < n_sp:
+            pl.when(sp >= step)(functools.partial(hand_on, step, c))
+
+    hand_on_if(1, 0)
     iota_r = lax.broadcasted_iota(jnp.int32, (rows, rows), 0)
     iota_c = lax.broadcasted_iota(jnp.int32, (rows, rows), 1)
     causal = iota_r >= iota_c
     strict = iota_c < iota_r
 
-    def st_copy():
-        return pltpu.make_async_remote_copy(
-            src_ref=st_out, dst_ref=st_in, send_sem=st_sem.at[0], recv_sem=st_sem.at[1],
+    def st_copy(h):
+        return pltpu.make_async_remote_copy(
+            src_ref=st_out.at[h], dst_ref=st_in.at[h],
+            send_sem=st_sem.at[h], recv_sem=st_sem.at[n_heads + h],
             device_id={"sp": lax.rem(sp + 1, n_sp)}, device_id_type=MESH,
         )
 
     lower = jnp.where(causal, 1.0, 0.0).astype(BF16)
     forget_pre = finish(2)
+    hand_on_if(1, 1)
     rec_i = finish(3)
     for h in range(n_heads):
         lanes = slice(h * LANES, (h + 1) * LANES)
@@ -225,10 +266,12 @@
         st_loc[h] = dot_tn(rec_i[:, lanes], fresh)
         dec[h] = jnp.broadcast_to(jnp.exp(last), dec.shape[1:])
 
-    @pl.when(jnp.logical_and(sp == 0, has_next))
-    def _():
-        st_out[...] = st_loc[...].astype(BF16)
-        st_copy().start()
+        @pl.when(jnp.logical_and(sp == 0, has_next))
+        def _(h=h):
+            st_out[h] = st_loc[h].astype(BF16)
+            st_copy(h).start()
+
+    hand_on_if(2, 0)
 
     qbuf[...] = finish(4)
     later = jnp.where(iota_r > iota_c, 1.0, 0.0).astype(BF16)
@@ -257,8 +300,15 @@
                 att[:, lanes] += value * jnp.exp(past)
                 run[h] = past + both[:, rows:]
 
+    def attend_if(step):
+        if step < n_sp:
+            @pl.when(sp >= step)
+            def _():
+                attend(sp - step, False)
+
     attend(sp, True)
-
+    attend_if(1)
+    hand_on_if(2, 1)
     rec_q = finish(5)
     for h in range(n_heads):
         lanes = slice(h * LANES, (h + 1) * LANES)
@@ -267,96 +317,112 @@
         scores = jnp.where(causal, dot_nt(decayed, kinv[:, lanes]), 0.0)
         loc[:, lanes] = dot_nn(scores.astype(BF16), rec_i[:, lanes])
 
+    attend_if(2)
+
     def block(step, carry):
-        slot = sp - step
         for c in range(2):
-            kv_copy(slot, c).wait_recv()
-
-            @pl.when(has_next)
-            def _(c=c):
-                kv_copy(slot, c).start()
-        attend(slot, False)
+            hand_on(step, c)
+        attend(sp - step, False)
         return carry
 
-    lax.fori_loop(1, sp + 1, block, 0)
+    lax.fori_loop(3, sp + 1, block, 0)
 
     def h_copy(df, c):
-        return pltpu.make_async_remote_copy(
-            src_ref=heads.at[c], dst_ref=hrecv.at[df - 1, c],
-            send_sem=h_send.at[(df - 1) * 2 + c], recv_sem=h_recv.at[(df - 1) * 2 + c],
+        index = (df - 1) * (1 + n_heads) + c
+        if c == 0:
+            source, target = heads.at[0], hrecv.at[df - 1, 0]
+        else:
+            lanes = pl.ds((c - 1) * LANES, LANES)
+            source, target = heads.at[1, :, lanes], hrecv.at[df - 1, 1, :, lanes]
+        return pltpu.make_async_remote_copy(
+            src_ref=source, dst_ref=target, send_sem=h_send.at[index], recv_sem=h_recv.at[index],
             device_id={"fs": fs_at(df)}, device_id_type=MESH,
         )
 
     heads[0] = att[...].astype(BF16)
     for df in range(1, n_fs):
         h_copy(df, 0).start()
-
-    @pl.when(has_prev)
-    def _():
-        st_copy().wait_recv()
-
-        @pl.when(has_next)
-        def _():
-            for h in range(n_heads):
-                st_out[h] = (st_in[h].astype(F32) * dec[h, 0:1, :] + st_loc[h]).astype(BF16)
-            st_copy().start()
-
-        for h in range(n_heads):
-            lanes = slice(h * LANES, (h + 1) * LANES)
-            loc[:, lanes] += dot_nt(qdec[:, lanes], st_in[h])
 
     for h in range(n_heads):
         lanes = slice(h * LANES, (h + 1) * LANES)
+
+        @pl.when(has_prev)
+        def _(h=h, lanes=lanes):
+            st_copy(h).wait_recv()
+
+            @pl.when(has_next)
+            def _():
+                st_out[h] = (st_in[h].astype(F32) * dec[h, 0:1, :] + st_loc[h]).astype(BF16)
+                st_copy(h).start()
+
+            loc[:, lanes] += dot_nt(qdec[:, lanes], st_in[h])
+
         raw = loc[:, lanes]
         norm = lax.rsqrt(jnp.mean(raw * raw, axis=1, keepdims=True) + norm_eps)
         heads[1, :, lanes] = (raw * norm * out_gain[...]).astype(BF16)
-    for df in range(1, n_fs):
-        h_copy(df, 1).start()
+        for df in range(1, n_fs):
+            h_copy(df, 1 + h).start()
 
     w_copies[N_PROJ].wait()
     w_copies[N_PROJ + 1].wait()
 
-    def pp_copy(df, dt):
-        index = df * (n_tp - 1) + dt - 1
+    half = out_cols // CHUNKS
+
+    def pp_copy(df, dt, k):
+        index = (df * (n_tp - 1) + dt - 1) * CHUNKS + k
         start = pl.multiple_of(tp_at(dt) * share, share)
         return pltpu.make_async_remote_copy(
-            src_ref=part.at[df, pl.ds(start, share)], dst_ref=precv2.at[dt - 1, df],
+            src_ref=part.at[df, k, pl.ds(start, share)], dst_ref=precv2.at[dt - 1, df, k],
             send_sem=pp_send.at[index], recv_sem=pp_recv.at[index],
             device_id={"tp": tp_at(dt)}, device_id_type=MESH,
         )
 
-    def m_copy(df):
-        return pltpu.make_async_remote_copy(
-            src_ref=mix.at[df - 1], dst_ref=mrecv.at[df - 1],
-            send_sem=m_send.at[df - 1], recv_sem=m_recv.at[df - 1],
+    def m_copy(df, k):
+        index = (df - 1) * CHUNKS + k
+        return pltpu.make_async_remote_copy(
+            src_ref=mix.at[df - 1, k], dst_ref=mrecv.at[df - 1, k],
+            send_sem=m_send.at[index], recv_sem=m_recv.at[index],
             device_id={"fs": fs_at(df)}, device_id_type=MESH,
         )
 
-    def project(df, first, second):
-        part[df] = (dot_nn(first, obuf[0]) + dot_nn(second, obuf[1])).astype(BF16)
+    def reduced(df, k):
+        value = part[df, k, pl.ds(pl.multiple_of(tp * share, share), share)].astype(F32)
         for dt in range(1, n_tp):
-            pp_copy(df, dt).start()
-
-    def reduced(df):
-        value = part[df, pl.ds(pl.multiple_of(tp * share, share), share)].astype(F32)
+            pp_copy(df, dt, k).wait_recv()
+            value = value + precv2[dt - 1, df, k].astype(F32)
+        return value.astype(BF16)
+
+    def columns(owner, k):
+        return pl.ds(pl.multiple_of(owner * out_cols + k * half, LANES), half)
+
+    for df in range(1, n_fs):
+        h_copy(df, 0).wait_recv()
+        for k in range(CHUNKS):
+            part_acc[df - 1, k] = dot_nn(hrecv[df - 1, 0], obuf[0, :, k * half:(k + 1) * half])
+    for k in range(CHUNKS):
+        cut = slice(k * half, (k + 1) * half)
+        part[0, k] = (dot_nn(heads[0], obuf[0, :, cut]) + dot_nn(heads[1], obuf[1, :, cut])).astype(BF16)
         for dt in range(1, n_tp):
-            pp_copy(df, dt).wait_recv()
-            value = value + precv2[dt - 1, df].astype(F32)
-        return value.astype(BF16)
-
-    project(0, heads[0], heads[1])
-    for df in range(1, n_fs):
-        h_copy(df, 0).wait_recv()
-        h_copy(df, 1).wait_recv()
-        project(df, hrecv[df - 1, 0], hrecv[df - 1, 1])
-    for df in range(1, n_fs):
-        mix[df - 1] = reduced(df)
-        m_copy(df).start()
-    out[:, pl.ds(pl.multiple_of(fs * out_cols, LANES), out_cols)] = reduced(0)
-    for df in range(1, n_fs):
-        m_copy(df).wait_recv()
+            pp_copy(0, dt, k).start()
+    for df in range(1, n_fs):
+        for h in range(n_heads):
+            h_copy(df, 1 + h).wait_recv()
+        for k in range(CHUNKS):
+            cut = slice(k * half, (k + 1) * half)
+            part[df, k] = (part_acc[df - 1, k] + dot_nn(hrecv[df - 1, 1], obuf[1, :, cut])).astype(BF16)
+            for dt in range(1, n_tp):
+                pp_copy(df, dt, k).start()
+    for df in range(1, n_fs):
+        for k in range(CHUNKS):
+            mix[df - 1, k] = reduced(df, k)
+            m_copy(df, k).start()
+    for k in range(CHUNKS):
+        out[:, columns(fs, k)] = reduced(0, k)
+    for df in range(1, n_fs):
         source = lax.rem(fs + n_fs - df, n_fs)
-        out[:, pl.ds(pl.multiple_of(source * out_cols, LANES), out_cols)] = mrecv[df - 1]
+        for k in range(CHUNKS):
+            m_copy(df, k).wait_recv()
+            out[:, columns(source, k)] = mrecv[df - 1, k]
 
     for df, dt in x_order:
         @pl.when(holder(fs_at(df)) == tp)
@@ -364,19 +430,24 @@
             x_copy(df, dt).wait_send()
     for dt in range(1, n_tp):
         ss_copy(dt).wait_send()
+        for df in range(1, n_fs):
+            f_copy(df, dt).wait_send()
     for df in range(1, n_fs):
         for w in range(N_PROJ):
             p_copy(df, w).wait_send()
-        for c in range(2):
+        for c in range(1 + n_heads):
             h_copy(df, c).wait_send()
-        m_copy(df).wait_send()
-    for df in range(n_fs):
-        for dt in range(1, n_tp):
-            pp_copy(df, dt).wait_send()
+    for k in range(CHUNKS):
+        for df in range(1, n_fs):
+            m_copy(df, k).wait_send()
+        for df in range(n_fs):
+            for dt in range(1, n_tp):
+                pp_copy(df, dt, k).wait_send()
 
     @pl.when(has_next)
     def _():
-        st_copy().wait_send()
+        for h in range(n_heads):
+            st_copy(h).wait_send()
 
         def drain(slot, carry):
             for c in range(2):
@@ -397,6 +468,7 @@
     n_heads = cols // LANES
     out_rows, out_cols = out_attn.shape
     share = rows // n_tp
+    piece = out_cols // CHUNKS
     vmem = pl.BlockSpec(memory_space=pltpu.VMEM)
     smem = pl.BlockSpec(memory_space=pltpu.SMEM)
     hbm = pl.BlockSpec(memory_space=pl.ANY)
@@ -405,9 +477,10 @@
     result = pl.pallas_call(
         functools.partial(kernel, n_sp, n_fs, n_tp),
         out_shape=jax.ShapeDtypeStruct((share, width), BF16),
-        in_specs=[vmem, vmem] + [hbm] * 6 + [smem, vmem, vmem, hbm, hbm],
+        in_specs=[hbm, vmem] + [hbm] * 6 + [smem, vmem, vmem, hbm, hbm],
         out_specs=vmem,
         scratch_shapes=[
+            pltpu.VMEM((rows, feat_t), BF16),
             pltpu.VMEM((N_PROJ, feat_f, cols), BF16),
             pltpu.VMEM((2, out_rows, out_cols), BF16),
             pltpu.VMEM((n_fs, rows, feat_f), BF16),
@@ -430,19 +503,20 @@
             pltpu.VMEM(square, BF16),
             pltpu.VMEM((2, rows, cols), BF16),
             pltpu.VMEM((n_fs - 1, 2, rows, cols), BF16),
-            pltpu.VMEM((n_fs, rows, out_cols), BF16),
-            pltpu.VMEM((n_tp - 1, n_fs, share, out_cols), BF16),
-            pltpu.VMEM((n_fs - 1, share, out_cols), BF16),
-            pltpu.VMEM((n_fs - 1, share, out_cols), BF16),
-            dma((N_PROJ + 2,)),
-            dma((n_fs * n_tp,)), dma((n_fs,)),
+            pltpu.VMEM((n_fs - 1, CHUNKS, rows, piece), F32),
+            pltpu.VMEM((n_fs, CHUNKS, rows, piece), BF16),
+            pltpu.VMEM((n_tp - 1, n_fs, CHUNKS, share, piece), BF16),
+            pltpu.VMEM((n_fs - 1, CHUNKS, share, piece), BF16),
+            pltpu.VMEM((n_fs - 1, CHUNKS, share, piece), BF16),
+            dma((1,)), dma((N_PROJ + 2,)),
+            dma((n_fs * n_tp,)), dma((n_fs * n_tp,)), dma((n_fs * n_tp,)),
             dma((n_tp - 1,)), dma((n_tp,)),
             dma(((n_fs - 1) * N_PROJ,)), dma(((n_fs - 1) * N_PROJ,)),
             dma((n_sp * 2,)), dma((n_sp * 2,)),
-            dma((2,)),
-            dma(((n_fs - 1) * 2,)), dma(((n_fs - 1) * 2,)),
-            dma((n_fs * (n_tp - 1),)), dma((n_fs * (n_tp - 1),)),
-            dma((n_fs - 1,)), dma((n_fs - 1,)),
+            dma((2 * n_heads,)),
+            dma(((n_fs - 1) * (1 + n_heads),)), dma(((n_fs - 1) * (1 + n_heads),)),
+            dma((n_fs * (n_tp - 1) * CHUNKS,)), dma((n_fs * (n_tp - 1) * CHUNKS,)),
+            dma(((n_fs - 1) * CHUNKS,)), dma(((n_fs - 1) * CHUNKS,)),
         ],
         compiler_params=pltpu.CompilerParams(
             collective_id=0, has_side_effects=True, vmem_limit_bytes=60 * 1024 * 1024

time: 56.5 us -> 49.7 us (0.88)
  Pallas kernels: 54.7 us -> 47.8 us
    pallas_call x1, Pallas kernels: 54.7 us -> 47.8 us  [body(): pl.pallas_call(functools.partial(kernel, n_sp, n_fs, n_tp), out_shape=jax...]
where the time goes in v2:
time: 49.7 us; the launch traced here: 49.5 us
  Pallas kernels  47.8 us (96%)
  local copies, waits for them, and re-layouts  1.67 us (3%)
    pallas_call x1, Pallas kernels, body(): pl.pallas_call(functools.partial(kernel, n_sp, n_fs, n_tp), out_shape=jax...  47.8 us
    unnamed x1, local copies, waits for them, and re-layouts  1.67 us

profile of v2, /device:TPU:29, one launch (start us, length us, event | category | flops | bytes accessed | tf_op | source)
XLA Modules:
  0.0 49.5 jit_solution(2333617426324622168)
XLA Ops:
  0.0 47.8 %layer.1 = bf16[64,2048]{1,0:T(8,128)(2,1)} custom-call(bf16[128,1024]{1,0:T(8,128)(2,1)} %bitcast.5, f32[1,2048]{1,0:T(1,128)} %bitcast.6, bf16[1024,512]{1,0:T(8,128)(2,1)} %w_k.1, bf16[1024,512]{1,0:T(8,128)(2,1)} %w_v.1, bf16[1024,512]{1,0:T(8,128)(2,1)} %w_f.1, bf16[1024,512]{1,0:T(8,128)(2,1)} %w_i.1, bf16[1024,512]{1,0:T(8,128)(2,1)} %w_q.1, ...), custom_call_target="tpu_custom_call" | custom-call | tf_op jit(solution)/shard_map/layer/pallas_call | solution.py:477
  47.8 1.7 %copy.15 = bf16[1,64,2048]{2,1,0:T(8,128)(2,1)} copy(bf16[1,64,2048]{2,1,0:T(8,128)(2,1)} %bitcast.4) | data formatting | bytes 524288

commit v3 on v2

--- a/solution.py
+++ b/solution.py
@@ -14,6 +14,7 @@
 F32 = jnp.float32
 BF16 = jnp.bfloat16
 N_PROJ = 6
+GROUPS = 2
 CHUNKS = 2
 
 
@@ -162,10 +163,18 @@
             device_id={"tp": tp_at(1)}, device_id_type=MESH,
         ).wait_recv()
 
-    def p_copy(df, w):
-        return pltpu.make_async_remote_copy(
-            src_ref=psend.at[df - 1, w], dst_ref=precv.at[df - 1, w],
-            send_sem=p_send.at[(df - 1) * N_PROJ + w], recv_sem=p_recv.at[(df - 1) * N_PROJ + w],
+    g_cols = cols // GROUPS
+    units = [(w, g * g_cols, g_cols) for g in range(GROUPS) for w in (0, 1)]
+    units += [(w, 0, cols) for w in range(2, N_PROJ)]
+    n_units = len(units)
+    n_kv = 2 * GROUPS
+
+    def p_copy(df, u):
+        w, first, count = units[u]
+        return pltpu.make_async_remote_copy(
+            src_ref=psend.at[df - 1, w, :, pl.ds(first, count)],
+            dst_ref=precv.at[df - 1, w, :, pl.ds(first, count)],
+            send_sem=p_send.at[(df - 1) * n_units + u], recv_sem=p_recv.at[(df - 1) * n_units + u],
             device_id={"fs": fs_at(df)}, device_id_type=MESH,
         )
 
@@ -180,11 +189,13 @@
             piece = tp_at(dt)
             x_wait(slot, piece, pl.multiple_of(piece * share, share), share)
         xg[df] = (xt[slot].astype(F32) * gain_f).astype(BF16)
-    for w in range(N_PROJ):
-        w_copies[w].wait()
+    for u, (w, first, count) in enumerate(units):
+        if first == 0:
+            w_copies[w].wait()
+        cut = slice(first, first + count)
         for df in range(1, n_fs):
-            psend[df - 1, w] = dot_nn(xg[df], wbuf[w]).astype(BF16)
-            p_copy(df, w).start()
+            psend[df - 1, w, :, cut] = dot_nn(xg[df], wbuf[w, :, cut]).astype(BF16)
+            p_copy(df, u).start()
 
     @pl.when(jnp.logical_not(own_holder))
     def _():
@@ -205,21 +216,23 @@
         total = total + ss[other]
     factor = lax.rsqrt(jnp.sum(total, axis=1, keepdims=True) / width + norm_eps)
 
-    def finish(w):
-        value = acc[w]
+    def finish(u):
+        w, first, count = units[u]
+        cut = slice(first, first + count)
+        value = acc[w, :, cut]
         for df in range(1, n_fs):
-            p_copy(df, w).wait_recv()
-            value = value + precv[df - 1, w].astype(F32)
+            p_copy(df, u).wait_recv()
+            value = value + precv[df - 1, w, :, cut].astype(F32)
         return (value * factor).astype(BF16)
 
     def kv_copy(slot, c):
         return pltpu.make_async_remote_copy(
             src_ref=kv.at[slot, c], dst_ref=kv.at[slot, c],
-            send_sem=kv_send.at[slot * 2 + c], recv_sem=kv_recv.at[slot * 2 + c],
+            send_sem=kv_send.at[slot * n_kv + c], recv_sem=kv_recv.at[slot * n_kv + c],
             device_id={"sp": lax.rem(sp + 1, n_sp)}, device_id_type=MESH,
         )
 
-    for c in range(2):
+    for c in range(n_kv):
         kv[sp, c] = finish(c)
 
         @pl.when(has_next)
@@ -238,6 +251,7 @@
             pl.when(sp >= step)(functools.partial(hand_on, step, c))
 
     hand_on_if(1, 0)
+    hand_on_if(1, 1)
     iota_r = lax.broadcasted_iota(jnp.int32, (rows, rows), 0)
     iota_c = lax.broadcasted_iota(jnp.int32, (rows, rows), 1)
     causal = iota_r >= iota_c
@@ -251,9 +265,10 @@
         )
 
     lower = jnp.where(causal, 1.0, 0.0).astype(BF16)
-    forget_pre = finish(2)
-    hand_on_if(1, 1)
-    rec_i = finish(3)
+    forget_pre = finish(n_kv)
+    for c in range(2, n_kv):
+        hand_on_if(1, c)
+    rec_i = finish(n_kv + 1)
     for h in range(n_heads):
         lanes = slice(h * LANES, (h + 1) * LANES)
         key_in = room[h:h + 1, :] * jax.nn.sigmoid(-forget_pre[:, lanes].astype(F32))
@@ -272,16 +287,20 @@
             st_copy(h).start()
 
     hand_on_if(2, 0)
-
-    qbuf[...] = finish(4)
+    hand_on_if(2, 1)
+
+    qbuf[...] = finish(n_kv + 2)
     later = jnp.where(iota_r > iota_c, 1.0, 0.0).astype(BF16)
     sums = jnp.concatenate([later, jnp.ones((rows, LANES), BF16)], axis=1)
     scale = 1.0 / math.sqrt(LANES)
 
-    def attend(slot, diagonal):
-        for h in range(n_heads):
+    g_heads = n_heads // GROUPS
+
+    def attend(slot, g, diagonal):
+        for h in range(g * g_heads, (g + 1) * g_heads):
             lanes = slice(h * LANES, (h + 1) * LANES)
-            z = dot_nt(qbuf[:, lanes], kv[slot, 0, :, lanes]) * scale + offs[h]
+            inner = slice((h - g * g_heads) * LANES, (h - g * g_heads + 1) * LANES)
+            z = dot_nt(qbuf[:, lanes], kv[slot, 2 * g, :, inner]) * scale + offs[h]
             keep = -(jnp.maximum(z, 0.0) + jnp.log1p(jnp.exp(-jnp.abs(z))))
             log_stick = z + keep
             if diagonal:
@@ -291,7 +310,7 @@
             stick = jnp.exp(log_stick + both[:, :rows])
             if diagonal:
                 stick = jnp.where(strict, stick, 0.0)
-            value = dot_nn(stick.astype(BF16), kv[slot, 1, :, lanes])
+            value = dot_nn(stick.astype(BF16), kv[slot, 2 * g + 1, :, inner])
             if diagonal:
                 att[:, lanes] = value
                 run[h] = both[:, rows:]
@@ -304,12 +323,15 @@
         if step < n_sp:
             @pl.when(sp >= step)
             def _():
-                attend(sp - step, False)
-
-    attend(sp, True)
+                for g in range(GROUPS):
+                    attend(sp - step, g, False)
+
+    for g in range(GROUPS):
+        attend(sp, g, True)
+    for c in range(2, n_kv):
+        hand_on_if(2, c)
     attend_if(1)
-    hand_on_if(2, 1)
-    rec_q = finish(5)
+    rec_q = finish(n_kv + 3)
     for h in range(n_heads):
         lanes = slice(h * LANES, (h + 1) * LANES)
         decayed = (rec_q[:, lanes].astype(F32) * ecum[:, lanes]).astype(BF16)
@@ -320,28 +342,40 @@
     attend_if(2)
 
     def block(step, carry):
-        for c in range(2):
+        for c in range(n_kv):
             hand_on(step, c)
-        attend(sp - step, False)
+        for g in range(GROUPS):
+            attend(sp - step, g, False)
         return carry
 
-    lax.fori_loop(3, sp + 1, block, 0)
+    lax.fori_loop(3, sp, block, 0)
+
+    n_head_units = GROUPS + n_heads
 
     def h_copy(df, c):
-        index = (df - 1) * (1 + n_heads) + c
-        if c == 0:
-            source, target = heads.at[0], hrecv.at[df - 1, 0]
+        index = (df - 1) * n_head_units + c
+        if c < GROUPS:
+            lanes = pl.ds(c * g_cols, g_cols)
+            source, target = heads.at[0, :, lanes], hrecv.at[df - 1, 0, :, lanes]
         else:
-            lanes = pl.ds((c - 1) * LANES, LANES)
+            lanes = pl.ds((c - GROUPS) * LANES, LANES)
             source, target = heads.at[1, :, lanes], hrecv.at[df - 1, 1, :, lanes]
         return pltpu.make_async_remote_copy(
             src_ref=source, dst_ref=target, send_sem=h_send.at[index], recv_sem=h_recv.at[index],
             device_id={"fs": fs_at(df)}, device_id_type=MESH,
         )
 
-    heads[0] = att[...].astype(BF16)
-    for df in range(1, n_fs):
-        h_copy(df, 0).start()
+    for g in range(GROUPS):
+        @pl.when(sp >= 3)
+        def _(g=g):
+            for c in (2 * g, 2 * g + 1):
+                hand_on(sp, c)
+            attend(0, g, False)
+
+        cut = slice(g * g_cols, (g + 1) * g_cols)
+        heads[0, :, cut] = att[:, cut].astype(BF16)
+        for df in range(1, n_fs):
+            h_copy(df, g).start()
 
     for h in range(n_heads):
         lanes = slice(h * LANES, (h + 1) * LANES)
@@ -361,7 +395,7 @@
         norm = lax.rsqrt(jnp.mean(raw * raw, axis=1, keepdims=True) + norm_eps)
         heads[1, :, lanes] = (raw * norm * out_gain[...]).astype(BF16)
         for df in range(1, n_fs):
-            h_copy(df, 1 + h).start()
+            h_copy(df, GROUPS + h).start()
 
     w_copies[N_PROJ].wait()
     w_copies[N_PROJ + 1].wait()
@@ -396,7 +430,8 @@
         return pl.ds(pl.multiple_of(owner * out_cols + k * half, LANES), half)
 
     for df in range(1, n_fs):
-        h_copy(df, 0).wait_recv()
+        for g in range(GROUPS):
+            h_copy(df, g).wait_recv()
         for k in range(CHUNKS):
             part_acc[df - 1, k] = dot_nn(hrecv[df - 1, 0], obuf[0, :, k * half:(k + 1) * half])
     for k in range(CHUNKS):
@@ -406,7 +441,7 @@
             pp_copy(0, dt, k).start()
     for df in range(1, n_fs):
         for h in range(n_heads):
-            h_copy(df, 1 + h).wait_recv()
+            h_copy(df, GROUPS + h).wait_recv()
         for k in range(CHUNKS):
             cut = slice(k * half, (k + 1) * half)
             part[df, k] = (part_acc[df - 1, k] + dot_nn(hrecv[df - 1, 1], obuf[1, :, cut])).astype(BF16)
@@ -433,9 +468,9 @@
         for df in range(1, n_fs):
             f_copy(df, dt).wait_send()
     for df in range(1, n_fs):
-        for w in range(N_PROJ):
-            p_copy(df, w).wait_send()
-        for c in range(1 + n_heads):
+        for u in range(n_units):
+            p_copy(df, u).wait_send()
+        for c in range(n_head_units):
             h_copy(df, c).wait_send()
     for k in range(CHUNKS):
         for df in range(1, n_fs):
@@ -450,7 +485,7 @@
             st_copy(h).wait_send()
 
         def drain(slot, carry):
-            for c in range(2):
+            for c in range(n_kv):
                 kv_copy(slot, c).wait_send()
             return carry
 
@@ -469,6 +504,7 @@
     out_rows, out_cols = out_attn.shape
     share = rows // n_tp
     piece = out_cols // CHUNKS
+    n_units = 2 * GROUPS + N_PROJ - 2
     vmem = pl.BlockSpec(memory_space=pltpu.VMEM)
     smem = pl.BlockSpec(memory_space=pltpu.SMEM)
     hbm = pl.BlockSpec(memory_space=pl.ANY)
@@ -489,7 +525,7 @@
             pltpu.VMEM((N_PROJ, rows, cols), F32),
             pltpu.VMEM((n_fs - 1, N_PROJ, rows, cols), BF16),
             pltpu.VMEM((n_fs - 1, N_PROJ, rows, cols), BF16),
-            pltpu.VMEM((n_sp, 2, rows, cols), BF16),
+            pltpu.VMEM((n_sp, 2 * GROUPS, rows, cols // GROUPS), BF16),
             pltpu.VMEM((rows, cols), BF16),
             pltpu.VMEM((rows, cols), BF16),
             pltpu.VMEM((rows, cols), F32),
@@ -511,10 +547,10 @@
             dma((1,)), dma((N_PROJ + 2,)),
             dma((n_fs * n_tp,)), dma((n_fs * n_tp,)), dma((n_fs * n_tp,)),
             dma((n_tp - 1,)), dma((n_tp,)),
-            dma(((n_fs - 1) * N_PROJ,)), dma(((n_fs - 1) * N_PROJ,)),
-            dma((n_sp * 2,)), dma((n_sp * 2,)),
+            dma(((n_fs - 1) * n_units,)), dma(((n_fs - 1) * n_units,)),
+            dma((n_sp * 2 * GROUPS,)), dma((n_sp * 2 * GROUPS,)),
             dma((2 * n_heads,)),
-            dma(((n_fs - 1) * (1 + n_heads),)), dma(((n_fs - 1) * (1 + n_heads),)),
+            dma(((n_fs - 1) * (GROUPS + n_heads),)), dma(((n_fs - 1) * (GROUPS + n_heads),)),
             dma((n_fs * (n_tp - 1) * CHUNKS,)), dma((n_fs * (n_tp - 1) * CHUNKS,)),
             dma(((n_fs - 1) * CHUNKS,)), dma(((n_fs - 1) * CHUNKS,)),
         ],

time: 49.7 us -> 47.9 us (0.964)
  Pallas kernels: 47.8 us -> 46.1 us
    pallas_call x1, Pallas kernels: 47.8 us -> 46.1 us  [body(): pl.pallas_call(functools.partial(kernel, n_sp, n_fs, n_tp), out_shape=jax...]
where the time goes in v3:
time: 47.9 us; the launch traced here: 47.8 us
  Pallas kernels  46.1 us (96%)
  local copies, waits for them, and re-layouts  1.67 us (3%)
    pallas_call x1, Pallas kernels, body(): pl.pallas_call(functools.partial(kernel, n_sp, n_fs, n_tp), out_shape=jax...  46.1 us
    unnamed x1, local copies, waits for them, and re-layouts  1.67 us

profile of v3, /device:TPU:29, one launch (start us, length us, event | category | flops | bytes accessed | tf_op | source)
XLA Modules:
  0.0 47.8 jit_solution(678822920831575912)
XLA Ops:
  0.0 46.1 %layer.1 = bf16[64,2048]{1,0:T(8,128)(2,1)} custom-call(bf16[128,1024]{1,0:T(8,128)(2,1)} %bitcast.5, f32[1,2048]{1,0:T(1,128)} %bitcast.6, bf16[1024,512]{1,0:T(8,128)(2,1)} %w_k.1, bf16[1024,512]{1,0:T(8,128)(2,1)} %w_v.1, bf16[1024,512]{1,0:T(8,128)(2,1)} %w_f.1, bf16[1024,512]{1,0:T(8,128)(2,1)} %w_i.1, bf16[1024,512]{1,0:T(8,128)(2,1)} %w_q.1, ...), custom_call_target="tpu_custom_call" | custom-call | tf_op jit(solution)/shard_map/layer/pallas_call | solution.py:513
  46.1 1.7 %copy.15 = bf16[1,64,2048]{2,1,0:T(8,128)(2,1)} copy(bf16[1,64,2048]{2,1,0:T(8,128)(2,1)} %bitcast.4) | data formatting | bytes 524288

commit v4 on v3

--- a/solution.py
+++ b/solution.py
@@ -178,18 +178,40 @@
             device_id={"fs": fs_at(df)}, device_id_type=MESH,
         )
 
+    def row_part(dt):
+        return pl.ds(pl.multiple_of(tp_at(dt) * share, share), share)
+
+    def first_copy(df, dt):
+        index = (n_fs - 1) * n_units + (df - 1) * n_tp + dt
+        return pltpu.make_async_remote_copy(
+            src_ref=psend.at[df - 1, 0, row_part(dt), pl.ds(0, g_cols)],
+            dst_ref=precv.at[df - 1, 0, row_part(dt), pl.ds(0, g_cols)],
+            send_sem=p_send.at[index], recv_sem=p_recv.at[index],
+            device_id={"fs": fs_at(df)}, device_id_type=MESH,
+        )
+
+    def first_part(df, dt):
+        mine = row_part(dt)
+        xg[df, mine, :] = (xt[fs_at(df), mine, :].astype(F32) * gain_f).astype(BF16)
+        psend[df - 1, 0, mine, 0:g_cols] = dot_nn(xg[df, mine, :], wbuf[0, :, 0:g_cols]).astype(BF16)
+        first_copy(df, dt).start()
+
+    w_copies[0].wait()
     for df in range(1, n_fs):
         slot = fs_at(df)
         x_wait(slot, tp, pl.multiple_of(tp * share, share), share)
         for dt in range(1, n_tp):
             f_copy(df, dt).start()
+        first_part(df, 0)
     for df in range(1, n_fs):
         slot = fs_at(df)
         for dt in range(1, n_tp):
             piece = tp_at(dt)
             x_wait(slot, piece, pl.multiple_of(piece * share, share), share)
-        xg[df] = (xt[slot].astype(F32) * gain_f).astype(BF16)
+            first_part(df, dt)
     for u, (w, first, count) in enumerate(units):
+        if u == 0:
+            continue
         if first == 0:
             w_copies[w].wait()
         cut = slice(first, first + count)
@@ -221,7 +243,11 @@
         cut = slice(first, first + count)
         value = acc[w, :, cut]
         for df in range(1, n_fs):
-            p_copy(df, u).wait_recv()
+            if u == 0:
+                for dt in range(n_tp):
+                    first_copy(df, dt).wait_recv()
+            else:
+                p_copy(df, u).wait_recv()
             value = value + precv[df - 1, w, :, cut].astype(F32)
         return (value * factor).astype(BF16)
 
@@ -468,7 +494,9 @@
         for df in range(1, n_fs):
             f_copy(df, dt).wait_send()
     for df in range(1, n_fs):
-        for u in range(n_units):
+        for dt in range(n_tp):
+            first_copy(df, dt).wait_send()
+        for u in range(1, n_units):
             p_copy(df, u).wait_send()
         for c in range(n_head_units):
             h_copy(df, c).wait_send()
@@ -547,7 +575,7 @@
             dma((1,)), dma((N_PROJ + 2,)),
             dma((n_fs * n_tp,)), dma((n_fs * n_tp,)), dma((n_fs * n_tp,)),
             dma((n_tp - 1,)), dma((n_tp,)),
-            dma(((n_fs - 1) * n_units,)), dma(((n_fs - 1) * n_units,)),
+            dma(((n_fs - 1) * (n_units + n_tp),)), dma(((n_fs - 1) * (n_units + n_tp),)),
             dma((n_sp * 2 * GROUPS,)), dma((n_sp * 2 * GROUPS,)),
             dma((2 * n_heads,)),
             dma(((n_fs - 1) * (GROUPS + n_heads),)), dma(((n_fs - 1) * (GROUPS + n_heads),)),

time: 47.9 us -> 47.2 us (0.985)
  Pallas kernels: 46.1 us -> 45.3 us
    pallas_call x1, Pallas kernels: 46.1 us -> 45.3 us  [body(): pl.pallas_call(functools.partial(kernel, n_sp, n_fs, n_tp), out_shape=jax...]
where the time goes in v4:
time: 47.2 us; the launch traced here: 47 us
  Pallas kernels  45.3 us (96%)
  local copies, waits for them, and re-layouts  1.67 us (4%)
    pallas_call x1, Pallas kernels, body(): pl.pallas_call(functools.partial(kernel, n_sp, n_fs, n_tp), out_shape=jax...  45.3 us
    unnamed x1, local copies, waits for them, and re-layouts  1.67 us

profile of v4, /device:TPU:29, one launch (start us, length us, event | category | flops | bytes accessed | tf_op | source)
XLA Modules:
  0.0 47.0 jit_solution(1768195455901803233)
XLA Ops:
  0.0 45.3 %layer.1 = bf16[64,2048]{1,0:T(8,128)(2,1)} custom-call(bf16[128,1024]{1,0:T(8,128)(2,1)} %bitcast.5, f32[1,2048]{1,0:T(1,128)} %bitcast.6, bf16[1024,512]{1,0:T(8,128)(2,1)} %w_k.1, bf16[1024,512]{1,0:T(8,128)(2,1)} %w_v.1, bf16[1024,512]{1,0:T(8,128)(2,1)} %w_f.1, bf16[1024,512]{1,0:T(8,128)(2,1)} %w_i.1, bf16[1024,512]{1,0:T(8,128)(2,1)} %w_q.1, ...), custom_call_target="tpu_custom_call" | custom-call | tf_op jit(solution)/shard_map/layer/pallas_call | solution.py:541
  45.3 1.7 %copy.15 = bf16[1,64,2048]{2,1,0:T(8,128)(2,1)} copy(bf16[1,64,2048]{2,1,0:T(8,128)(2,1)} %bitcast.4) | data formatting | bytes 524288

commit v5 on v4

--- a/solution.py
+++ b/solution.py
@@ -224,7 +224,7 @@
         x_wait(fs, holder(fs), 0, rows)
         xg[0] = (xt[fs].astype(F32) * gain_f).astype(BF16)
 
-    for w in range(N_PROJ):
+    for w in range(2):
         acc[w] = dot_nn(xg[0], wbuf[w])
 
     total = ss[tp]
@@ -264,6 +264,9 @@
         @pl.when(has_next)
         def _(c=c):
             kv_copy(sp, c).start()
+
+    for w in range(2, N_PROJ):
+        acc[w] = dot_nn(xg[0], wbuf[w])
 
     def hand_on(step, c):
         kv_copy(sp - step, c).wait_recv()

time: 47.2 us -> 47.4 us (level)
  no operation moved by 1% of the time
where the time goes in v5:
time: 47.4 us; the launch traced here: 47.2 us
  Pallas kernels  45.5 us (96%)
  local copies, waits for them, and re-layouts  1.67 us (4%)
    pallas_call x1, Pallas kernels, body(): pl.pallas_call(functools.partial(kernel, n_sp, n_fs, n_tp), out_shape=jax...  45.5 us
    unnamed x1, local copies, waits for them, and re-layouts  1.67 us

profile of v5, /device:TPU:29, one launch (start us, length us, event | category | flops | bytes accessed | tf_op | source)
XLA Modules:
  0.0 47.2 jit_solution(8194415368613102354)
XLA Ops:
  0.0 45.5 %layer.1 = bf16[64,2048]{1,0:T(8,128)(2,1)} custom-call(bf16[128,1024]{1,0:T(8,128)(2,1)} %bitcast.5, f32[1,2048]{1,0:T(1,128)} %bitcast.6, bf16[1024,512]{1,0:T(8,128)(2,1)} %w_k.1, bf16[1024,512]{1,0:T(8,128)(2,1)} %w_v.1, bf16[1024,512]{1,0:T(8,128)(2,1)} %w_f.1, bf16[1024,512]{1,0:T(8,128)(2,1)} %w_i.1, bf16[1024,512]{1,0:T(8,128)(2,1)} %w_q.1, ...), custom_call_target="tpu_custom_call" | custom-call | tf_op jit(solution)/shard_map/layer/pallas_call | solution.py:544
  45.5 1.7 %copy.15 = bf16[1,64,2048]{2,1,0:T(8,128)(2,1)} copy(bf16[1,64,2048]{2,1,0:T(8,128)(2,1)} %bitcast.4) | data formatting | bytes 524288
